TPU v7x, 256 devices: a whole 4x4x8 slice. The times are simulated.
256 devices in a mesh: sp: 32 (over z, y), tp: 8 (over x, core).
Axes of the slice: x: 4, y: 4, z: 8, core: 2. Of those that a mesh axis runs over, the one named last changes fastest.
Arguments:
- tokens: bfloat16 [4, 16384, 2048], P(None, ('sp', 'tp')), may hold values from -6 to 6
- in_gain: float32 [2048], replicated, may hold values from 0.1 to 1.9
- query_weight: bfloat16 [2048, 1024], P(None, 'tp'), may hold values from -0.125 to 0.125
- key_weight: bfloat16 [2048, 1024], P(None, 'tp'), may hold values from -0.125 to 0.125
- value_weight: bfloat16 [2048, 1024], P(None, 'tp'), may hold values from -0.125 to 0.125
- gate_weight: bfloat16 [2048, 1024], P(None, 'tp'), may hold values from -0.125 to 0.125
- log_decay: float32 [8], P('tp'), may hold values from -0.034 to 0, as said below
- norm_gain: float32 [1024], P('tp'), may hold values from 0.1 to 1.9
- out_weight: bfloat16 [1024, 2048], replicated, may hold values from -0.1875 to 0.1875
- post_gain: float32 [2048], replicated, may hold values from 0.1 to 1.9
Outputs:
- mixed: bfloat16 [4, 16384, 2048], P(None, ('sp', 'tp'))
Inputs may be any that keep to these rules, and one draw needn't show every extreme that they name: `log_decay`: every entry is negative; some heads keep a tenth or more of their memory over 16384 positions, others lose most of it within 30 to 100 positions.
All inputs are finite; a program needn't handle non-finite values.
Results may differ from a plain program's by a relative error of at most 0.015.
Values may be sent and summed in bfloat16 or wider, within the bound.
A program may use at most 64 MiB of HBM per device.

v0:
```python
import functools
import math

import jax
import jax.numpy as jnp
import numpy as np
from jax import lax
from jax.experimental import pallas as pl
from jax.experimental.pallas import tpu as pltpu
from jax.sharding import PartitionSpec as P

HEAD_DIM = 128
SUB = 128
rms_eps = 1e-06
group_eps = 1e-05
rope_base = 10000.0
MESH = pl.DeviceIdType.MESH
F32 = jnp.float32
BF16 = jnp.bfloat16


def kernel(
    tp, sp,
    tok, gain_h, wq_h, wk_h, wv_h, wg_h, decay, ngain_h, wo_h, pgain_h, inv_h,
    out,
    gain, ngain, pgain, inv, gath, wq, wk, wv, wg, wo, nb, cosv, sinv, mask, qs, ks, vs, gs,
    within, state, excl, st_out, st_in, g_out, g_in, premix,
    x_send, p_send, t_recv, s_send, s_recv, g_send, g_recv, w_sem, own_sem,
):
    seqs, rows, width = tok.shape
    length = rows * tp
    cols = wq.shape[1]
    heads = cols // HEAD_DIM
    chips = tp // 2
    pair = 2 * rows
    rounds = [1 << k for k in range(max(1, (sp - 1).bit_length()))] if sp > 1 else []
    last = len(rounds) - 1
    s, t = lax.axis_index("sp"), lax.axis_index("tp")
    chip, core = lax.div(t, 2), lax.rem(t, 2)
    other = chip * 2 + 1 - core

    barrier = pltpu.get_barrier_semaphore()
    for j in range(1, tp):
        pl.semaphore_signal(
            barrier, inc=1, device_id={"tp": lax.rem(t + j, tp)}, device_id_type=MESH
        )
    for d in rounds:
        @pl.when(s + d < sp)
        def _():
            pl.semaphore_signal(barrier, inc=1, device_id={"sp": s + d}, device_id_type=MESH)

        @pl.when(s >= d)
        def _():
            pl.semaphore_signal(barrier, inc=1, device_id={"sp": s - d}, device_id_type=MESH)

    peers = jnp.int32(tp - 1)
    for d in rounds:
        peers = peers + jnp.where(s + d < sp, 1, 0) + jnp.where(s >= d, 1, 0)
    pl.semaphore_wait(barrier, peers)

    def block(q, who):
        return gath.at[q, pl.ds(pl.multiple_of(who * rows, rows), rows), :]

    def to_chip(q, j):
        peer = lax.rem(chip + j, chips) * 2 + core
        return pltpu.make_async_remote_copy(
            tok.at[q], block(q, t), x_send.at[q, j], t_recv.at[q, t],
            device_id={"tp": peer}, device_id_type=MESH,
        )

    def to_core(q, who, mine):
        return pltpu.make_async_remote_copy(
            tok.at[q] if mine else block(q, who), block(q, who),
            p_send.at[q, who], t_recv.at[q, who],
            device_id={"tp": other}, device_id_type=MESH,
        )

    def arrived(q, who):
        pltpu.make_async_remote_copy(
            tok.at[q], block(q, who), p_send.at[q, who], t_recv.at[q, who],
            device_id={"tp": other}, device_id_type=MESH,
        ).wait_recv()

    for q in range(seqs):
        for j in range(1, chips):
            to_chip(q, j).start()
    own = [pltpu.make_async_copy(tok.at[q], block(q, t), own_sem.at[q]) for q in range(seqs)]
    for q in range(seqs):
        own[q].start()
        to_core(q, t, True).start()
    loads = [
        pltpu.make_async_copy(a, b, w_sem.at[i])
        for i, (a, b) in enumerate(
            (
                (inv_h, inv), (gain_h, gain), (ngain_h, ngain), (pgain_h, pgain),
                (wk_h, wk), (wv_h, wv), (wq_h, wq), (wg_h, wg), (wo_h, wo),
            )
        )
    ]
    for load in loads:
        load.start()

    loads[0].wait()
    place = (s * length + lax.broadcasted_iota(jnp.int32, (length, HEAD_DIM), 0)).astype(F32)
    angle = place * inv[...]
    cosv[...] = jnp.cos(angle)
    lane = lax.broadcasted_iota(jnp.int32, (length, HEAD_DIM), 1)
    sine = jnp.sin(angle)
    sinv[...] = jnp.where(lane < HEAD_DIM // 2, -sine, sine)
    for h in range(heads):
        def fill(i, _):
            at = pl.multiple_of(i * 32, 32)
            gap = (
                at + lax.broadcasted_iota(jnp.int32, (32, length), 0)
                - lax.broadcasted_iota(jnp.int32, (32, length), 1)
            )
            weight = jnp.exp(decay[h] * jnp.maximum(gap, 0).astype(F32))
            mask[h, pl.ds(at, 32), :] = jnp.where(gap >= 0, weight, 0.0)
            return 0

        lax.fori_loop(0, length // 32, fill, 0)
    excl[...] = jnp.zeros_like(excl)

    def head(h):
        return slice(h * HEAD_DIM, (h + 1) * HEAD_DIM)

    def normalise(q, who):
        base = pl.multiple_of(who * rows, rows)

        def norm(i, _):
            at = pl.multiple_of(base + i * 16, 16)
            x = gath[q, pl.ds(at, 16), :].astype(F32)
            scale = lax.rsqrt(jnp.mean(x * x, axis=-1, keepdims=True) + rms_eps)
            nb[pl.ds(at, 16), :] = (x * scale * gain[...]).astype(BF16)
            return 0

        lax.fori_loop(0, rows // 16, norm, 0, unroll=2)

    def project(q, which, parts):
        span = pl.ds(pl.multiple_of(which * pair, pair), pair)
        for w, dest, kind in parts:
            r = jnp.dot(nb[span, :], w[...], preferred_element_type=F32).astype(BF16)
            if kind == 0:
                dest[q, span, :] = r
            else:
                for h in range(heads):
                    x = r[:, head(h)].astype(F32)
                    x = x * cosv[span, :] + pltpu.roll(x, HEAD_DIM // 2, 1) * sinv[span, :]
                    if kind == 2:
                        x = x * HEAD_DIM ** (-0.5)
                    dest[q, span, head(h)] = x.astype(BF16)

    first = ((wk, ks, 2), (wv, vs, 0))
    second = ((wq, qs, 1), (wg, gs, 0))

    def send_state(q, k):
        for h in range(heads):
            total = state[q, h] + jnp.exp(jnp.full((1, 1), decay[h] * length, F32)) * excl[q, h]
            st_out[q, k, h] = total.astype(BF16)

        @pl.when(s + rounds[k] < sp)
        def _():
            state_copy(q, k).start()

    def state_copy(q, k):
        return pltpu.make_async_remote_copy(
            st_out.at[q, k], st_in.at[q, k], s_send.at[q, k], s_recv.at[q, k],
            device_id={"sp": lax.rem(s + rounds[k], sp)}, device_id_type=MESH,
        )

    def take_state(q, k):
        @pl.when(s >= rounds[k])
        def _():
            state_copy(q, k).wait_recv()
            for h in range(heads):
                rate = jnp.exp(jnp.full((1, 1), decay[h] * (length * (rounds[k] - 1)), F32))
                excl[q, h] += rate * st_in[q, k, h].astype(F32)

    def make_state(q):
        spot = lax.broadcasted_iota(jnp.int32, (length, HEAD_DIM), 0)
        for h in range(heads):
            fade = jnp.exp(decay[h] * (length - 1 - spot).astype(F32))
            scaled = (ks[q, :, head(h)].astype(F32) * fade).astype(BF16)
            state[q, h] = lax.dot_general(
                scaled, vs[q, :, head(h)], (((0,), (0,)), ((), ())), preferred_element_type=F32
            )

    def inside(q):
        for h in range(heads):
            for i in range(length // SUB):
                here, upto = slice(i * SUB, (i + 1) * SUB), slice(0, (i + 1) * SUB)
                score = lax.dot_general(
                    qs[q, here, head(h)], ks[q, upto, head(h)],
                    (((1,), (1,)), ((), ())), preferred_element_type=F32,
                )
                weight = (score * mask[h, here, upto]).astype(BF16)
                within[q, here, head(h)] = jnp.dot(
                    weight, vs[q, upto, head(h)], preferred_element_type=F32
                )

    def gated_copy(q, dest, source):
        return pltpu.make_async_remote_copy(
            g_out.at[q, pl.ds(pl.multiple_of(dest * rows, rows), rows), :],
            g_in.at[q, :, pl.ds(pl.multiple_of(source * cols, cols), cols)],
            g_send.at[q, dest], g_recv.at[q, source],
            device_id={"tp": dest}, device_id_type=MESH,
        )

    def gated_own(q):
        return pltpu.make_async_copy(
            g_out.at[q, pl.ds(pl.multiple_of(t * rows, rows), rows), :],
            g_in.at[q, :, pl.ds(pl.multiple_of(t * cols, cols), cols)],
            g_recv.at[q, t],
        )

    def members(j):
        base = lax.rem(chip + j, chips) * 2
        return base + core, base + 1 - core

    def finish(q):
        for dest in [d for j in range(1, chips) for d in members(j)] + [other, t]:
            here = pl.ds(pl.multiple_of(dest * rows, rows), rows)
            spot = dest * rows + 1 + lax.broadcasted_iota(jnp.int32, (rows, HEAD_DIM), 0)
            for h in range(heads):
                reach = jnp.exp(decay[h] * spot.astype(F32))
                query = (qs[q, here, head(h)].astype(F32) * reach).astype(BF16)
                kept = within[q, here, head(h)] + jnp.dot(
                    query, excl[q, h].astype(BF16), preferred_element_type=F32
                )
                kept = kept - jnp.mean(kept, axis=-1, keepdims=True)
                spread = jnp.mean(kept * kept, axis=-1, keepdims=True)
                normal = kept * lax.rsqrt(spread + group_eps) * ngain[:, head(h)]
                gate = gs[q, here, head(h)].astype(F32)
                g_out[q, here, head(h)] = (normal * (gate * jax.nn.sigmoid(gate))).astype(BF16)
            if dest is t:
                gated_own(q).start()
            else:
                gated_copy(q, dest, t).start()

    def emit(q):
        step = min(512, width)
        for j in range(chips):
            if j == 0:
                gated_own(q).wait()
                gated_copy(q, other, other).wait_recv()
            else:
                for source in members(j):
                    gated_copy(q, other, source).wait_recv()
            span = pl.ds(pl.multiple_of(lax.rem(chip + j, chips) * 2 * cols, 2 * cols), 2 * cols)
            for c in range(width // step):
                part = slice(c * step, (c + 1) * step)
                term = jnp.dot(g_in[q, :, span], wo[span, part], preferred_element_type=F32)
                premix[:, part] = term if j == 0 else premix[:, part] + term

        def norm(i, _):
            at = pl.multiple_of(i * 16, 16)
            x = premix[pl.ds(at, 16), :]
            scale = lax.rsqrt(jnp.mean(x * x, axis=-1, keepdims=True) + rms_eps)
            out[q, pl.ds(at, 16), :] = (x * scale * pgain[...]).astype(BF16)
            return 0

        lax.fori_loop(0, rows // 16, norm, 0, unroll=2)

    for q in range(seqs):
        own[q].wait()
    for load in loads[1:]:
        load.wait()

    def near(q, _):
        normalise(q, t)
        arrived(q, other)
        normalise(q, other)
        project(q, chip, first + second)
        return 0

    lax.fori_loop(0, seqs, near, 0)

    def far(q, _):
        for j in range(1, chips):
            mine, _ = members(j)
            arrived(q, mine)
            to_core(q, mine, False).start()
        if last > 0:
            @pl.when(q > 0)
            def _():
                for k in range(1, last):
                    take_state(q - 1, k)
                    send_state(q - 1, k + 1)
        for j in range(1, chips):
            mine, theirs = members(j)
            normalise(q, mine)
            arrived(q, theirs)
            normalise(q, theirs)
            project(q, lax.rem(chip + j, chips), first)
        make_state(q)
        if rounds:
            send_state(q, 0)
        for j in range(1, chips):
            project(q, lax.rem(chip + j, chips), second)
        if last > 0:
            take_state(q, 0)
            send_state(q, 1)
        inside(q)

        @pl.when(q > 0)
        def _():
            if last >= 0:
                take_state(q - 1, last)
            finish(q - 1)
        return 0

    lax.fori_loop(0, seqs, far, 0)

    def write(q, _):
        emit(q)
        return 0

    end = seqs - 1
    for k in range(1, last):
        take_state(end, k)
        send_state(end, k + 1)
    done = min(2, end)
    lax.fori_loop(0, done, write, 0)
    if last >= 0:
        take_state(end, last)
    finish(end)

    lax.fori_loop(done, seqs, write, 0)

    def drain(q, _):
        for j in range(1, chips):
            to_chip(q, j).wait_send()
            to_core(q, lax.rem(chip + j, chips) * 2 + core, False).wait_send()
        to_core(q, t, True).wait_send()
        for j in range(1, tp):
            gated_copy(q, lax.rem(t + j, tp), t).wait_send()
        for k, d in enumerate(rounds):
            @pl.when(s + d < sp)
            def _():
                state_copy(q, k).wait_send()
        return 0

    lax.fori_loop(0, seqs, drain, 0)


def hand_over(source, out, held, in_sem, out_sem):
    pieces = range(source.shape[0])
    into = [pltpu.make_async_copy(source.at[i], held.at[i], in_sem.at[i]) for i in pieces]
    back = [pltpu.make_async_copy(held.at[i], out.at[i], out_sem.at[i]) for i in pieces]
    for copy in into:
        copy.start()
    for i in pieces:
        into[i].wait()
        back[i].start()
    for copy in back:
        copy.wait()


def solution(mesh):
    tp, sp = mesh.shape["tp"], mesh.shape["sp"]

    def body(tok, gain, wq, wk, wv, wg, decay, ngain, wo, pgain):
        seqs, rows, width = tok.shape
        cols = wq.shape[1]
        heads = cols // HEAD_DIM
        length = rows * tp
        half = HEAD_DIM // 2
        inv = np.float32(rope_base) ** (-np.arange(half, dtype=np.float32) / half)
        inv = jnp.asarray(np.concatenate([inv, inv])[None, :], F32)
        steps = max(1, (sp - 1).bit_length())
        dma = pltpu.SemaphoreType.DMA
        hbm, vmem = pl.BlockSpec(memory_space=pltpu.HBM), pl.BlockSpec(memory_space=pltpu.VMEM)
        wide = pltpu.VMEM((seqs, length, cols), BF16)
        mixed = pl.pallas_call(
            functools.partial(kernel, tp, sp),
            out_shape=jax.ShapeDtypeStruct(tok.shape, BF16),
            in_specs=[
                hbm, hbm, hbm, hbm, hbm, hbm,
                pl.BlockSpec(memory_space=pltpu.SMEM), hbm, hbm, hbm, hbm,
            ],
            out_specs=vmem,
            scratch_shapes=[
                pltpu.VMEM((1, width), F32), pltpu.VMEM((1, cols), F32),
                pltpu.VMEM((1, width), F32), pltpu.VMEM((1, HEAD_DIM), F32),
                pltpu.VMEM((seqs, length, width), BF16),
                pltpu.VMEM(wq.shape, BF16), pltpu.VMEM(wq.shape, BF16),
                pltpu.VMEM(wq.shape, BF16), pltpu.VMEM(wq.shape, BF16),
                pltpu.VMEM(wo.shape, BF16),
                pltpu.VMEM((length, width), BF16),
                pltpu.VMEM((length, HEAD_DIM), F32), pltpu.VMEM((length, HEAD_DIM), F32),
                pltpu.VMEM((heads, length, length), F32),
                wide, wide, wide, wide,
                pltpu.VMEM((seqs, length, cols), F32),
                pltpu.VMEM((seqs, heads, HEAD_DIM, HEAD_DIM), F32),
                pltpu.VMEM((seqs, heads, HEAD_DIM, HEAD_DIM), F32),
                pltpu.VMEM((seqs, steps, heads, HEAD_DIM, HEAD_DIM), BF16),
                pltpu.VMEM((seqs, steps, heads, HEAD_DIM, HEAD_DIM), BF16),
                wide,
                pltpu.VMEM((seqs, rows, cols * tp), BF16),
                pltpu.VMEM((rows, width), F32),
                dma((seqs, max(2, tp // 2))), dma((seqs, tp)), dma((seqs, tp)),
                dma((seqs, steps)), dma((seqs, steps)),
                dma((seqs, tp)), dma((seqs, tp)),
                dma((9,)), dma((seqs,)),
            ],
            compiler_params=pltpu.CompilerParams(
                collective_id=0, has_side_effects=True, vmem_limit_bytes=59 * 2**20
            ),
            name="retention",
        )(
            tok, gain[None, :], wq, wk, wv, wg, decay, ngain[None, :], wo, pgain[None, :], inv
        )
        return pl.pallas_call(
            hand_over,
            out_shape=jax.ShapeDtypeStruct(tok.shape, BF16),
            in_specs=[hbm],
            out_specs=hbm,
            scratch_shapes=[pltpu.VMEM(tok.shape, BF16), dma((seqs,)), dma((seqs,))],
            compiler_params=pltpu.CompilerParams(vmem_limit_bytes=59 * 2**20),
            name="hand_over",
        )(mixed)

    placed = (
        P(None, ("sp", "tp"), None),
        P(),
        P(None, "tp"),
        P(None, "tp"),
        P(None, "tp"),
        P(None, "tp"),
        P("tp"),
        P("tp"),
        P(),
        P(),
    )
    return jax.shard_map(
        body, mesh=mesh, in_specs=placed, out_specs=P(None, ("sp", "tp"), None), check_vma=False
    )
```

profile of v0, /device:TPU:227, one launch (start us, length us, event | category | flops | bytes accessed | tf_op | source)
XLA Modules:
  0.0 90.7 jit_solution(17994328697488036280)
XLA Ops:
  0.7 88.1 %retention.1.source = bf16[4,64,2048]{2,1,0:T(8,128)(2,1)} custom-call(bf16[4,64,2048]{2,1,0:T(8,128)(2,1)} %tok.1, f32[1,2048]{1,0:T(1,128)} %bitcast.3, bf16[2048,128]{1,0:T(8,128)(2,1)} %wq_h.1, bf16[2048,128]{1,0:T(8,128)(2,1)} %wk_h.1, bf16[2048,128]{1,0:T(8,128)(2,1)} %wv_h.1, bf16[2048,128]{1,0:T(8,128)(2,1)} %wg_h.1, f32[1]{0:T(128)S(6)} %copy.12.decay, ...), custom_call_target="tpu_custom_call" | custom-call | tf_op jit(solution)/shard_map/retention/pallas_call | solution.py:374
  88.7 2.0 %hand_over.1 = bf16[4,64,2048]{2,1,0:T(8,128)(2,1)} custom-call(bf16[4,64,2048]{2,1,0:T(8,128)(2,1)} %retention.1.source), custom_call_target="tpu_custom_call" | custom-call | tf_op jit(solution)/shard_map/hand_over/pallas_call | solution.py:413
where the time goes:
time: 91.7 us; the launch traced here: 90.7 us
  Pallas kernels  90.1 us (98%)
    pallas_call x1, Pallas kernels, body(): pl.pallas_call(functools.partial(kernel, tp, sp), out_shape=jax.ShapeDtyp...  88.1 us
    pallas_call x1, Pallas kernels, body(): pl.pallas_call(hand_over, out_shape=jax.ShapeDtypeStruct(tok.shape, BF16)...  1.98 us

commit v1 on v0

v1 whole, which is shorter than its diff:
```python
import functools

import jax
import jax.numpy as jnp
import numpy as np
from jax import lax
from jax.experimental import pallas as pl
from jax.experimental.pallas import tpu as pltpu
from jax.sharding import PartitionSpec as P

HEAD_DIM = 128
SUB = 128
NY = 4
rms_eps = 1e-06
group_eps = 1e-05
rope_base = 10000.0
MESH = pl.DeviceIdType.MESH
F32 = jnp.float32
BF16 = jnp.bfloat16


def kernel(
    tp, sp,
    tok, gain_h, wq_h, wk_h, wv_h, wg_h, decay, ngain_h, wo_h, pgain_h, inv_h,
    out,
    gain, ngain, pgain, inv, tokv, gath, wkv, wqg, wo, cosv, sinv, mask, qs, ks, vs, gs,
    within, s1_out, s1_in, s2_out, s2_in, s3_out, carry, excl, g_out, g_in, premix, outv,
    x_send, p_send, t_recv, s1_send, s1_recv, s2_send, s2_recv, s3_send, s3_recv,
    g_send, g_recv, w_sem, in_sem, o_sem,
):
    seqs, rows, width = tok.shape
    length = rows * tp
    chips = tp // 2
    pair = 2 * rows
    nz = sp // NY
    part = HEAD_DIM // NY
    s, t = lax.axis_index("sp"), lax.axis_index("tp")
    z, y = lax.div(s, NY), lax.rem(s, NY)
    chip, core = lax.div(t, 2), lax.rem(t, 2)
    other = chip * 2 + 1 - core
    left, right, far = lax.rem(chip + 3, chips), lax.rem(chip + 1, chips), lax.rem(chip + 2, chips)
    relay_from, relay_to = lax.rem(chip + 3 + 2 * core, chips), lax.rem(chip + 1 + 2 * core, chips)

    loads_in = [pltpu.make_async_copy(tok.at[q], tokv.at[q], in_sem.at[q]) for q in range(seqs)]
    for load in loads_in:
        load.start()
    halves = (slice(0, HEAD_DIM), slice(HEAD_DIM, 2 * HEAD_DIM))
    loads = [
        pltpu.make_async_copy(a, b, w_sem.at[i])
        for i, (a, b) in enumerate(
            (
                (gain_h, gain), (inv_h, inv), (ngain_h, ngain), (pgain_h, pgain),
                (wk_h, wkv.at[:, halves[0]]), (wv_h, wkv.at[:, halves[1]]),
                (wq_h, wqg.at[:, halves[0]]), (wg_h, wqg.at[:, halves[1]]), (wo_h, wo),
            )
        )
    ]
    for load in loads:
        load.start()

    barrier = pltpu.get_barrier_semaphore()
    for j in range(1, tp):
        pl.semaphore_signal(
            barrier, inc=1, device_id={"tp": lax.rem(t + j, tp)}, device_id_type=MESH
        )
    for j in range(1, NY):
        pl.semaphore_signal(
            barrier, inc=1, device_id={"sp": z * NY + lax.rem(y + j, NY)}, device_id_type=MESH
        )
    for j in range(1, nz):
        pl.semaphore_signal(
            barrier, inc=1, device_id={"sp": lax.rem(z + j, nz) * NY + y}, device_id_type=MESH
        )

    def at_rows(who, n):
        return pl.ds(pl.multiple_of(who * n, n), n)

    loads[0].wait()
    for load in loads_in:
        load.wait()

    def normalise(i, _):
        q, at = lax.div(i, rows // 16), pl.multiple_of(lax.rem(i, rows // 16) * 16, 16)
        x = tokv[q, pl.ds(at, 16), :].astype(F32)
        scale = lax.rsqrt(jnp.mean(x * x, axis=-1, keepdims=True) + rms_eps)
        gath[q, pl.ds(pl.multiple_of(t * rows + at, 16), 16), :] = (x * scale * gain[...]).astype(BF16)
        return 0

    lax.fori_loop(0, seqs * (rows // 16), normalise, 0, unroll=2)
    pl.semaphore_wait(barrier, tp - 1 + NY - 1 + nz - 1)

    def block_copy(q, who, dest, sem):
        return pltpu.make_async_remote_copy(
            gath.at[q, at_rows(who, rows), :], gath.at[q, at_rows(who, rows), :],
            sem, t_recv.at[q, who], device_id={"tp": dest}, device_id_type=MESH,
        )

    def to_right(q):
        return block_copy(q, t, right * 2 + core, x_send.at[q, 0])

    def to_left(q):
        return block_copy(q, t, left * 2 + core, x_send.at[q, 1])

    def relay(q):
        return block_copy(q, relay_from * 2 + core, relay_to * 2 + core, x_send.at[q, 2])

    def to_core(q, k):
        return block_copy(q, k * 2 + core, other, p_send.at[q, k])

    def arrived(q, who):
        block_copy(q, who, other, x_send.at[q, 0]).wait_recv()

    def send_own(q):
        to_right(q).start()
        to_left(q).start()
        to_core(q, chip).start()

    send_own(0)
    send_own(1)

    loads[1].wait()
    place = (s * length + lax.broadcasted_iota(jnp.int32, (length, HEAD_DIM), 0)).astype(F32)
    angle = place * inv[...]
    cosv[...] = jnp.cos(angle)
    lane = lax.broadcasted_iota(jnp.int32, (length, HEAD_DIM), 1)
    sine = jnp.sin(angle)
    sinv[...] = jnp.where(lane < HEAD_DIM // 2, -sine, sine)

    def fill(i, _):
        at = pl.multiple_of(i * 32, 32)
        gap = (
            at + lax.broadcasted_iota(jnp.int32, (32, length), 0)
            - lax.broadcasted_iota(jnp.int32, (32, length), 1)
        )
        weight = jnp.exp(decay[0] * jnp.maximum(gap, 0).astype(F32))
        mask[pl.ds(at, 32), :] = jnp.where(gap >= 0, weight, 0.0)
        return 0

    lax.fori_loop(0, length // 32, fill, 0)
    for load in loads[2:]:
        load.wait()

    def rotate(x, span):
        x = x.astype(BF16).astype(F32)
        return x * cosv[span, :] + pltpu.roll(x, HEAD_DIM // 2, 1) * sinv[span, :]

    def project_kv(q, k):
        span = at_rows(k, pair)
        r = jnp.dot(gath[q, span, :], wkv[...], preferred_element_type=F32)
        ks[q, span, :] = (rotate(r[:, halves[0]], span) * HEAD_DIM ** (-0.5)).astype(BF16)
        vs[q, span, :] = r[:, halves[1]].astype(BF16)

    def project_qg(q, k):
        span = at_rows(k, pair)
        r = jnp.dot(gath[q, span, :], wqg[...], preferred_element_type=F32)
        qs[q, span, :] = rotate(r[:, halves[0]], span).astype(BF16)
        gs[q, span, :] = r[:, halves[1]].astype(BF16)

    def power(n):
        return jnp.exp(jnp.full((1, 1), decay[0] * n, F32))

    def s1_copy(q, j):
        peer = lax.rem(y + j, NY)
        return pltpu.make_async_remote_copy(
            s1_out.at[q, at_rows(peer, part), :], s1_in.at[q, y],
            s1_send.at[q, j], s1_recv.at[q, y],
            device_id={"sp": z * NY + peer}, device_id_type=MESH,
        )

    def s1_wait(q, j):
        peer = lax.rem(y + j, NY)
        pltpu.make_async_remote_copy(
            s1_out.at[q, at_rows(peer, part), :], s1_in.at[q, peer],
            s1_send.at[q, j], s1_recv.at[q, peer],
            device_id={"sp": z * NY + peer}, device_id_type=MESH,
        ).wait_recv()

    def make_state(q):
        spot = lax.broadcasted_iota(jnp.int32, (length, HEAD_DIM), 0)
        fade = jnp.exp(decay[0] * (length - 1 - spot).astype(F32))
        scaled = (ks[q].astype(F32) * fade).astype(BF16)
        total = lax.dot_general(
            scaled, vs[q], (((0,), (0,)), ((), ())), preferred_element_type=F32
        )
        s1_out[q] = total.astype(BF16)
        for j in range(1, NY):
            s1_copy(q, j).start()
        s1_in[q, y] = s1_out[q, at_rows(y, part), :]

    def s2_copy(q, d):
        return pltpu.make_async_remote_copy(
            s2_out.at[q], s2_in.at[q, d], s2_send.at[q, d], s2_recv.at[q, d],
            device_id={"sp": lax.rem(z + d, nz) * NY + y}, device_id_type=MESH,
        )

    def plane_total(q):
        for j in range(1, NY):
            s1_wait(q, j)
        step = power(length)
        total = s1_in[q, 0].astype(F32)
        for k in range(1, NY):
            total = total * step + s1_in[q, k].astype(F32)
        s2_out[q] = total.astype(BF16)
        for d in range(1, nz):
            @pl.when(z + d < nz)
            def _():
                s2_copy(q, d).start()

    def s3_copy(q, j):
        peer = lax.rem(y + j, NY)
        return pltpu.make_async_remote_copy(
            s3_out.at[q, peer], excl.at[q, at_rows(y, part), :],
            s3_send.at[q, j], s3_recv.at[q, y],
            device_id={"sp": z * NY + peer}, device_id_type=MESH,
        )

    def s3_wait(q, j):
        peer = lax.rem(y + j, NY)
        pltpu.make_async_remote_copy(
            s3_out.at[q, peer], excl.at[q, at_rows(peer, part), :],
            s3_send.at[q, j], s3_recv.at[q, peer],
            device_id={"sp": z * NY + peer}, device_id_type=MESH,
        ).wait_recv()

    def hand_back(q):
        carry[...] = jnp.zeros_like(carry)
        for d in range(1, nz):
            @pl.when(z >= d)
            def _():
                s2_copy(q, d).wait_recv()
                carry[...] += power(length * NY * (d - 1)) * s2_in[q, d].astype(F32)
        step = power(length)
        before = carry[...]
        for k in range(NY):
            s3_out[q, k] = before.astype(BF16)
            before = before * step + s1_in[q, k].astype(F32)
        for j in range(1, NY):
            s3_copy(q, j).start()
        excl[q, at_rows(y, part), :] = s3_out[q, y]

    def inside(q):
        for i in range(length // SUB):
            here, upto = slice(i * SUB, (i + 1) * SUB), slice(0, (i + 1) * SUB)
            score = lax.dot_general(
                qs[q, here, :], ks[q, upto, :],
                (((1,), (1,)), ((), ())), preferred_element_type=F32,
            )
            weight = (score * mask[here, upto]).astype(BF16)
            within[q, here, :] = jnp.dot(weight, vs[q, upto, :], preferred_element_type=F32)

    def gated_copy(q, dest, source):
        return pltpu.make_async_remote_copy(
            g_out.at[q, at_rows(dest, rows), :],
            g_in.at[q, :, at_rows(source, HEAD_DIM)],
            g_send.at[q, dest], g_recv.at[q, source],
            device_id={"tp": dest}, device_id_type=MESH,
        )

    def finish(q):
        for j in range(1, NY):
            s3_wait(q, j)
        memory = excl[q]
        for k in (far, left, right, chip):
            here = at_rows(k, pair)
            spot = k * pair + 1 + lax.broadcasted_iota(jnp.int32, (pair, HEAD_DIM), 0)
            reach = jnp.exp(decay[0] * spot.astype(F32))
            query = (qs[q, here, :].astype(F32) * reach).astype(BF16)
            kept = within[q, here, :] + jnp.dot(query, memory, preferred_element_type=F32)
            kept = kept - jnp.mean(kept, axis=-1, keepdims=True)
            spread = jnp.mean(kept * kept, axis=-1, keepdims=True)
            normal = kept * lax.rsqrt(spread + group_eps) * ngain[...]
            gate = gs[q, here, :].astype(F32)
            g_out[q, here, :] = (normal * (gate * jax.nn.sigmoid(gate))).astype(BF16)
            if k is chip:
                gated_copy(q, other, t).start()
                g_in[q, :, at_rows(t, HEAD_DIM)] = g_out[q, at_rows(t, rows), :]
            else:
                gated_copy(q, k * 2 + core, t).start()
                gated_copy(q, k * 2 + 1 - core, t).start()

    def gated_wait(q):
        for j in range(1, tp):
            source = lax.rem(t + j, tp)
            gated_copy(q, other, source).wait_recv()

    def emit(lo, hi):
        n = (hi - lo) * rows
        for q in range(lo, hi):
            gated_wait(q)
        step = 512
        g = g_in[lo:hi].reshape(n, g_in.shape[2])
        for c in range(width // step):
            cut = slice(c * step, (c + 1) * step)
            premix[0:n, cut] = jnp.dot(g, wo[:, cut], preferred_element_type=F32)

        def norm(i, _):
            at = pl.multiple_of(i * 16, 16)
            x = premix[pl.ds(at, 16), :]
            scale = lax.rsqrt(jnp.mean(x * x, axis=-1, keepdims=True) + rms_eps)
            q = lo + lax.div(i, rows // 16)
            to = pl.multiple_of(lax.rem(i, rows // 16) * 16, 16)
            outv[q, pl.ds(to, 16), :] = (x * scale * pgain[...]).astype(BF16)
            return 0

        lax.fori_loop(0, n // 16, norm, 0, unroll=2)
        for q in range(lo, hi):
            pltpu.make_async_copy(outv.at[q], out.at[q], o_sem.at[q]).start()

    def take(q):
        arrived(q, relay_from * 2 + core)
        relay(q).start()

    def spread_on(q):
        to_core(q, relay_from).start()
        arrived(q, relay_to * 2 + core)
        to_core(q, relay_to).start()

    def near(q):
        arrived(q, other)
        project_kv(q, chip)
        project_qg(q, chip)
        arrived(q, left * 2 + 1 - core)
        project_kv(q, left)
        project_qg(q, left)
        arrived(q, right * 2 + 1 - core)
        project_kv(q, right)
        project_qg(q, right)

    take(0)
    send_own(2)
    spread_on(0)
    near(0)

    def step(q, _):
        @pl.when(q < seqs - 1)
        def _():
            take(q + 1)

            @pl.when(q < seqs - 3)
            def _():
                send_own(q + 3)

            spread_on(q + 1)

        arrived(q, far * 2 + core)
        to_core(q, far).start()

        @pl.when(q > 0)
        def _():
            hand_back(q - 1)

        arrived(q, far * 2 + 1 - core)
        project_kv(q, far)
        make_state(q)
        project_qg(q, far)
        inside(q)

        @pl.when(q < seqs - 1)
        def _():
            plane_total(q)
            near(q + 1)
        return 0

    lax.fori_loop(0, seqs, step, 0)
    end = seqs - 1
    finish(0)
    plane_total(end)

    def rest(q, _):
        finish(q)
        return 0

    lax.fori_loop(1, end, rest, 0)
    hand_back(end)
    emit(0, end)
    finish(end)
    emit(end, seqs)

    def drain(q, _):
        to_right(q).wait_send()
        to_left(q).wait_send()
        relay(q).wait_send()
        for k in range(chips):
            to_core(q, k).wait_send()
        for j in range(1, NY):
            s1_copy(q, j).wait_send()
            s3_copy(q, j).wait_send()
        for d in range(1, nz):
            @pl.when(z + d < nz)
            def _():
                s2_copy(q, d).wait_send()
        for j in range(1, tp):
            gated_copy(q, lax.rem(t + j, tp), t).wait_send()
        return 0

    lax.fori_loop(0, seqs, drain, 0)
    for q in range(seqs):
        pltpu.make_async_copy(outv.at[q], out.at[q], o_sem.at[q]).wait()


def hand_over(source, out, held, in_sem, out_sem):
    pieces = range(source.shape[0])
    into = [pltpu.make_async_copy(source.at[i], held.at[i], in_sem.at[i]) for i in pieces]
    back = [pltpu.make_async_copy(held.at[i], out.at[i], out_sem.at[i]) for i in pieces]
    for copy in into:
        copy.start()
    for i in pieces:
        into[i].wait()
        back[i].start()
    for copy in back:
        copy.wait()


def solution(mesh):
    tp, sp = mesh.shape["tp"], mesh.shape["sp"]

    def body(tok, gain, wq, wk, wv, wg, decay, ngain, wo, pgain):
        seqs, rows, width = tok.shape
        cols = wq.shape[1]
        length = rows * tp
        nz = sp // NY
        part = HEAD_DIM // NY
        half = HEAD_DIM // 2
        inv = np.float32(rope_base) ** (-np.arange(half, dtype=np.float32) / half)
        inv = jnp.asarray(np.concatenate([inv, inv])[None, :], F32)
        dma = pltpu.SemaphoreType.DMA
        hbm = pl.BlockSpec(memory_space=pltpu.HBM)
        vmem = pltpu.VMEM
        wide = vmem((seqs, length, cols), BF16)
        mixed = pl.pallas_call(
            functools.partial(kernel, tp, sp),
            out_shape=jax.ShapeDtypeStruct(tok.shape, BF16),
            in_specs=[
                hbm, hbm, hbm, hbm, hbm, hbm,
                pl.BlockSpec(memory_space=pltpu.SMEM), hbm, hbm, hbm, hbm,
            ],
            out_specs=hbm,
            scratch_shapes=[
                vmem((1, width), F32), vmem((1, cols), F32),
                vmem((1, width), F32), vmem((1, HEAD_DIM), F32),
                vmem(tok.shape, BF16),
                vmem((seqs, length, width), BF16),
                vmem((width, 2 * cols), BF16), vmem((width, 2 * cols), BF16),
                vmem(wo.shape, BF16),
                vmem((length, HEAD_DIM), F32), vmem((length, HEAD_DIM), F32),
                vmem((length, length), F32),
                wide, wide, wide, wide,
                vmem((seqs, length, cols), F32),
                vmem((seqs, HEAD_DIM, HEAD_DIM), BF16),
                vmem((seqs, NY, part, HEAD_DIM), BF16),
                vmem((seqs, part, HEAD_DIM), BF16),
                vmem((seqs, nz, part, HEAD_DIM), BF16),
                vmem((seqs, NY, part, HEAD_DIM), BF16),
                vmem((part, HEAD_DIM), F32),
                vmem((seqs, HEAD_DIM, HEAD_DIM), BF16),
                wide,
                vmem((seqs, rows, cols * tp), BF16),
                vmem((seqs * rows, width), F32),
                vmem(tok.shape, BF16),
                dma((seqs, 3)), dma((seqs, tp)), dma((seqs, tp)),
                dma((seqs, NY)), dma((seqs, NY)), dma((seqs, nz)), dma((seqs, nz)),
                dma((seqs, NY)), dma((seqs, NY)),
                dma((seqs, tp)), dma((seqs, tp)),
                dma((9,)), dma((seqs,)), dma((seqs,)),
            ],
            compiler_params=pltpu.CompilerParams(
                collective_id=0, has_side_effects=True, vmem_limit_bytes=59 * 2**20
            ),
            name="retention",
        )(
            tok, gain[None, :], wq, wk, wv, wg, decay, ngain[None, :], wo, pgain[None, :], inv
        )
        return pl.pallas_call(
            hand_over,
            out_shape=jax.ShapeDtypeStruct(tok.shape, BF16),
            in_specs=[hbm],
            out_specs=hbm,
            scratch_shapes=[pltpu.VMEM(tok.shape, BF16), dma((seqs,)), dma((seqs,))],
            compiler_params=pltpu.CompilerParams(vmem_limit_bytes=59 * 2**20),
            name="hand_over",
        )(mixed)

    placed = (
        P(None, ("sp", "tp"), None),
        P(),
        P(None, "tp"),
        P(None, "tp"),
        P(None, "tp"),
        P(None, "tp"),
        P("tp"),
        P("tp"),
        P(),
        P(),
    )
    return jax.shard_map(
        body, mesh=mesh, in_specs=placed, out_specs=P(None, ("sp", "tp"), None), check_vma=False
    )
```

time: 91.7 us -> 76.3 us (0.83)
  the two profiles are of different devices: /device:TPU:227 before, /device:TPU:1 now
where the time goes in v1:
time: 76.3 us; the launch traced here: 76.1 us
  Pallas kernels  75.5 us (99%)
    pallas_call x1, Pallas kernels, body(): pl.pallas_call(functools.partial(kernel, tp, sp), out_shape=jax.ShapeDtyp...  73.5 us
    pallas_call x1, Pallas kernels, body(): pl.pallas_call(hand_over, out_shape=jax.ShapeDtypeStruct(tok.shape, BF16)...  1.98 us

profile of v1, /device:TPU:1, one launch (start us, length us, event | category | flops | bytes accessed | tf_op | source)
XLA Modules:
  0.0 76.1 jit_solution(1807143872216449813)
XLA Ops:
  0.7 73.5 %retention.1.source = bf16[4,64,2048]{2,1,0:T(8,128)(2,1)} custom-call(bf16[4,64,2048]{2,1,0:T(8,128)(2,1)} %tok.1, f32[1,2048]{1,0:T(1,128)} %bitcast.3, bf16[2048,128]{1,0:T(8,128)(2,1)} %wq_h.1, bf16[2048,128]{1,0:T(8,128)(2,1)} %wk_h.1, bf16[2048,128]{1,0:T(8,128)(2,1)} %wv_h.1, bf16[2048,128]{1,0:T(8,128)(2,1)} %wg_h.1, f32[1]{0:T(128)S(6)} %copy.12.decay, ...), custom_call_target="tpu_custom_call" | custom-call | tf_op jit(solution)/shard_map/retention/pallas_call | solution.py:430
  74.2 2.0 %hand_over.1 = bf16[4,64,2048]{2,1,0:T(8,128)(2,1)} custom-call(bf16[4,64,2048]{2,1,0:T(8,128)(2,1)} %retention.1.source), custom_call_target="tpu_custom_call" | custom-call | tf_op jit(solution)/shard_map/hand_over/pallas_call | solution.py:473

commit v2 on v1

v2 whole, which is shorter than its diff:
```python
import functools

import jax
import jax.numpy as jnp
import numpy as np
from jax import lax
from jax.experimental import pallas as pl
from jax.experimental.pallas import tpu as pltpu
from jax.sharding import PartitionSpec as P

HEAD_DIM = 128
SUB = 128
NY = 4
rms_eps = 1e-06
group_eps = 1e-05
rope_base = 10000.0
MESH = pl.DeviceIdType.MESH
F32 = jnp.float32
BF16 = jnp.bfloat16


def kernel(
    tp, sp,
    tok, gain_h, wq_h, wk_h, wv_h, wg_h, decay, ngain_h, wo_h, pgain_h, inv_h,
    out,
    gain, pgain, inv, heads, tokv, gath, w, wo, cosv, sinv, mask, fade, reach,
    qs, qr, ks, vs, sg, within, s1_out, s1_in, s2_out, s2_in, s3_out, carry, excl,
    g_out, g_in, premix, outv,
    x_send, p_send, t_recv, wx_send, wx_recv, wy_send, wy_recv, h_send, h_recv,
    s1_send, s1_recv, s2_send, s2_recv, s3_send, s3_recv, g_send, g_recv,
    w_sem, o_sem, in_sem, out_sem,
):
    seqs, rows, width = tok.shape
    pair = 2 * rows
    length = 2 * pair
    line = rows * tp
    nz = sp // NY
    part = HEAD_DIM // NY
    direct = width // 4
    piece = (width - direct) // NY
    s, t = lax.axis_index("sp"), lax.axis_index("tp")
    z, y = lax.div(s, NY), lax.rem(s, NY)
    chip, core = lax.div(t, 2), lax.rem(t, 2)
    group, side = lax.div(chip, 2), lax.rem(chip, 2)
    base = group * 4
    me = side * 2 + core
    twin = side * 2 + 1 - core
    across = (1 - side) * 2 + core
    across_twin = (1 - side) * 2 + 1 - core
    mirror = (3 - chip) * 2 + core
    slot = y * 2 + group

    loads_in = [pltpu.make_async_copy(tok.at[q], tokv.at[q], in_sem.at[q]) for q in range(seqs)]
    cuts = [slice(i * HEAD_DIM, (i + 1) * HEAD_DIM) for i in range(4)]
    loads_w = [
        pltpu.make_async_copy(a, w.at[0, :, cuts[i]], w_sem.at[i])
        for i, a in enumerate((wk_h, wv_h, wq_h, wg_h))
    ]
    loads = [
        pltpu.make_async_copy(a, b, w_sem.at[4 + i])
        for i, (a, b) in enumerate(
            ((ngain_h, heads.at[0, 1:2, :]), (gain_h, gain), (inv_h, inv), (pgain_h, pgain))
        )
    ]

    def head_of(u, flip):
        c = group * 2 + u // 2
        return ((3 - c) if flip else c) * 2 + u % 2

    loads_o = [
        pltpu.make_async_copy(
            wo_h.at[pl.ds(pl.multiple_of(head_of(i // 2, i % 2) * HEAD_DIM, HEAD_DIM), HEAD_DIM), :],
            wo.at[i * HEAD_DIM:(i + 1) * HEAD_DIM, :], o_sem.at[i],
        )
        for i in range(8)
    ]
    for load in loads_w + loads_in + loads + loads_o:
        load.start()

    barrier = pltpu.get_barrier_semaphore()

    def greet(dest):
        pl.semaphore_signal(barrier, inc=1, device_id=dest, device_id_type=MESH)

    for u in (twin, across, across_twin):
        greet({"tp": base + u})
    for j in range(1, NY):
        greet({"sp": z * NY + lax.rem(y + j, NY)})
    for j in range(NY):
        greet({"sp": z * NY + lax.rem(y + j, NY), "tp": mirror})
    for j in range(1, nz):
        greet({"sp": lax.rem(z + j, nz) * NY + y})

    def at_rows(who, n):
        return pl.ds(pl.multiple_of(who * n, n), n)

    def cross(i):
        span = pl.ds(pl.multiple_of(direct + y * piece, 128), piece)
        return pltpu.make_async_remote_copy(
            w.at[0, span, cuts[i]], w.at[1, span, cuts[i]], wx_send.at[0, i], wx_recv.at[0, i],
            device_id={"tp": mirror}, device_id_type=MESH,
        )

    def straight(i):
        return pltpu.make_async_remote_copy(
            w.at[0, 0:direct, cuts[i]], w.at[1, 0:direct, cuts[i]],
            wx_send.at[1, i], wx_recv.at[1, i],
            device_id={"tp": mirror}, device_id_type=MESH,
        )

    def along(i, j, mine):
        peer = lax.rem(y + j, NY)
        owner = y if mine else peer
        span = pl.ds(pl.multiple_of(direct + owner * piece, 128), piece)
        return pltpu.make_async_remote_copy(
            w.at[1, span, cuts[i]], w.at[1, span, cuts[i]], wy_send.at[i, j], wy_recv.at[i, owner],
            device_id={"sp": z * NY + peer}, device_id_type=MESH,
        )

    def pass_on(i):
        cross(i).wait_recv()
        for j in range(1, NY):
            along(i, j, True).start()

    def have(i):
        straight(i).wait_recv()
        for j in range(1, NY):
            along(i, j, False).wait_recv()

    def head_copy():
        return pltpu.make_async_remote_copy(
            heads.at[0], heads.at[1], h_send, h_recv, device_id={"tp": mirror}, device_id_type=MESH,
        )

    loads[0].wait()
    heads[0, 0:1, :] = jnp.full((1, HEAD_DIM), decay[0], F32)
    for load in loads_w:
        load.wait()
    with jax.named_scope("barrier"):
        pl.semaphore_wait(barrier, 3 + NY - 1 + NY + nz - 1)
    for i in range(4):
        cross(i).start()
    for i in range(4):
        straight(i).start()
    head_copy().start()

    def block_copy(q, u, dest, sem):
        return pltpu.make_async_remote_copy(
            gath.at[q, at_rows(u, rows), :], gath.at[q, at_rows(u, rows), :],
            sem, t_recv.at[q, u], device_id={"tp": base + dest}, device_id_type=MESH,
        )

    def to_across(q):
        return block_copy(q, me, across, x_send.at[q])

    def to_twin(q, own):
        return block_copy(q, me if own else across, twin, p_send.at[q, 0 if own else 1])

    def arrived(q, u):
        block_copy(q, u, twin, x_send.at[q]).wait_recv()

    def normalise(q):
        def norm(i, _):
            at = pl.multiple_of(i * 16, 16)
            x = tokv[q, pl.ds(at, 16), :].astype(F32)
            scale = lax.rsqrt(jnp.mean(x * x, axis=-1, keepdims=True) + rms_eps)
            to = pl.ds(pl.multiple_of(me * rows + at, 16), 16)
            gath[q, to, :] = (x * scale * gain[...]).astype(BF16)
            return 0

        lax.fori_loop(0, rows // 16, norm, 0, unroll=2)

    def send(q):
        to_across(q).start()
        to_twin(q, True).start()

    with jax.named_scope("norm"):
        loads[1].wait()
        for q in range(seqs):
            loads_in[q].wait()
            normalise(q)
            if q > 0:
                send(q - 1)
        send(seqs - 1)

    with jax.named_scope("tables"):
        loads[2].wait()
        place = s * line + group * length + lax.broadcasted_iota(jnp.int32, (length, HEAD_DIM), 0)
        angle = place.astype(F32) * inv[...]
        cosv[...] = jnp.cos(angle)
        lane = lax.broadcasted_iota(jnp.int32, (length, HEAD_DIM), 1)
        sine = jnp.sin(angle)
        sinv[...] = jnp.where(lane < HEAD_DIM // 2, -sine, sine)

    def tables(h):
        rate = heads[h, 0:1, :]
        spot = lax.broadcasted_iota(jnp.int32, (length, HEAD_DIM), 0)
        fade[h] = jnp.exp(rate * (length - 1 - spot).astype(F32))
        reach[h] = jnp.exp(rate * (1 + spot).astype(F32))
        for c in range(length // HEAD_DIM):
            gap = spot - c * HEAD_DIM - lax.broadcasted_iota(jnp.int32, (length, HEAD_DIM), 1)
            weight = jnp.exp(rate * jnp.maximum(gap, 0).astype(F32))
            mask[h, :, c * HEAD_DIM:(c + 1) * HEAD_DIM] = jnp.where(gap >= 0, weight, 0.0)

    with jax.named_scope("tables0"):
        tables(0)

    def rotate(x, span):
        x = x.astype(BF16).astype(F32)
        return x * cosv[span, :] + pltpu.roll(x, HEAD_DIM // 2, 1) * sinv[span, :]

    def project_kv(h, q, span):
        r = jnp.dot(gath[q, span, :], w[h, :, 0:256], preferred_element_type=F32)
        ks[h, q, span, :] = (rotate(r[:, cuts[0]], span) * HEAD_DIM ** (-0.5)).astype(BF16)
        vs[h, q, span, :] = r[:, cuts[1]].astype(BF16)

    def project_qg(h, q, span):
        r = jnp.dot(gath[q, span, :], w[h, :, 256:512], preferred_element_type=F32)
        query = rotate(r[:, cuts[0]], span).astype(BF16)
        qs[h, q, span, :] = query
        qr[h, q, span, :] = (query.astype(F32) * reach[h, span, :]).astype(BF16)
        gate = r[:, cuts[1]].astype(BF16).astype(F32)
        sg[h, q, span, :] = heads[h, 1:2, :] * (gate * jax.nn.sigmoid(gate))

    everything = slice(0, length)
    own_rows = at_rows(side, pair)
    far_rows = at_rows(1 - side, pair)

    def power(n):
        return jnp.exp(jnp.full((1, 1), decay[0] * n, F32))

    def s1_copy(q, h, j, mine):
        peer = lax.rem(y + j, NY)
        dest = {"sp": z * NY + peer, "tp": mirror} if h else {"sp": z * NY + peer}
        arrival = slot if mine else peer * 2 + (1 - group if h else group)
        return pltpu.make_async_remote_copy(
            s1_out.at[h, q, at_rows(peer, part), :], s1_in.at[q, arrival],
            s1_send.at[h, q, j], s1_recv.at[q, arrival], device_id=dest, device_id_type=MESH,
        )

    def make_state(q):
        for h in range(2):
            scaled = (ks[h, q].astype(F32) * fade[h]).astype(BF16)
            total = lax.dot_general(
                scaled, vs[h, q], (((0,), (0,)), ((), ())), preferred_element_type=F32
            )
            s1_out[h, q] = total.astype(BF16)
        for j in range(NY):
            s1_copy(q, 1, j, True).start()
            if j:
                s1_copy(q, 0, j, True).start()
        s1_in[q, slot] = s1_out[0, q, at_rows(y, part), :]

    def s2_copy(q, d):
        return pltpu.make_async_remote_copy(
            s2_out.at[q], s2_in.at[q, d], s2_send.at[q, d], s2_recv.at[q, d],
            device_id={"sp": lax.rem(z + d, nz) * NY + y}, device_id_type=MESH,
        )

    def plane_total(q):
        for j in range(NY):
            s1_copy(q, 1, j, False).wait_recv()
            if j:
                s1_copy(q, 0, j, False).wait_recv()
        step = power(length)
        total = s1_in[q, 0].astype(F32)
        for k in range(1, 2 * NY):
            total = total * step + s1_in[q, k].astype(F32)
        s2_out[q] = total.astype(BF16)
        for d in range(1, nz):
            @pl.when(z + d < nz)
            def _():
                s2_copy(q, d).start()

    def s3_copy(q, h, j, mine):
        peer = lax.rem(y + j, NY)
        dest = {"sp": z * NY + peer, "tp": mirror} if h else {"sp": z * NY + peer}
        owner = y if mine else peer
        return pltpu.make_async_remote_copy(
            s3_out.at[q, peer * 2 + (1 - group if h else group)],
            excl.at[h, q, at_rows(owner, part), :],
            s3_send.at[h, q, j], s3_recv.at[h, q, owner], device_id=dest, device_id_type=MESH,
        )

    def hand_back(q):
        carry[...] = jnp.zeros_like(carry)
        for d in range(1, nz):
            @pl.when(z >= d)
            def _():
                s2_copy(q, d).wait_recv()
                carry[...] += power(line * NY * (d - 1)) * s2_in[q, d].astype(F32)
        step = power(length)
        before = carry[...]
        for k in range(2 * NY):
            s3_out[q, k] = before.astype(BF16)
            before = before * step + s1_in[q, k].astype(F32)
        for j in range(NY):
            s3_copy(q, 1, j, True).start()
            if j:
                s3_copy(q, 0, j, True).start()
        excl[0, q, at_rows(y, part), :] = s3_out[q, slot]

    def inside(q):
        for h in range(2):
            for i in range(length // SUB):
                here, upto = slice(i * SUB, (i + 1) * SUB), slice(0, (i + 1) * SUB)
                score = lax.dot_general(
                    qs[h, q, here, :], ks[h, q, upto, :],
                    (((1,), (1,)), ((), ())), preferred_element_type=F32,
                )
                weight = (score * mask[h, here, upto]).astype(BF16)
                within[h, q, here, :] = jnp.dot(
                    weight, vs[h, q, upto, :], preferred_element_type=F32
                )

    def gated_copy(q, dest, source):
        return pltpu.make_async_remote_copy(
            g_out.at[q, at_rows(dest, rows), :], g_in.at[q, :, at_rows(source, 2 * HEAD_DIM)],
            g_send.at[q, dest], g_recv.at[q, source],
            device_id={"tp": base + dest}, device_id_type=MESH,
        )

    def finish(q):
        for j in range(NY):
            s3_copy(q, 1, j, False).wait_recv()
            if j:
                s3_copy(q, 0, j, False).wait_recv()
        for k in range(2):
            here = at_rows((1 - side) if k == 0 else side, pair)
            for h in range(2):
                kept = within[h, q, here, :] + jnp.dot(
                    qr[h, q, here, :], excl[h, q], preferred_element_type=F32
                )
                kept = kept - jnp.mean(kept, axis=-1, keepdims=True)
                spread = jnp.mean(kept * kept, axis=-1, keepdims=True)
                normal = kept * lax.rsqrt(spread + group_eps) * sg[h, q, here, :]
                g_out[q, here, cuts[h]] = normal.astype(BF16)
            if k == 0:
                gated_copy(q, across, me).start()
                gated_copy(q, across_twin, me).start()
            else:
                gated_copy(q, twin, me).start()
                g_in[q, :, at_rows(me, 2 * HEAD_DIM)] = g_out[q, at_rows(me, rows), :]

    def gated_wait(q):
        for u in (twin, across, across_twin):
            gated_copy(q, twin, u).wait_recv()

    def emit(lo, hi):
        n = (hi - lo) * rows
        with jax.named_scope("gated_wait"):
            for q in range(lo, hi):
                gated_wait(q)
        step = 512
        g = g_in[lo:hi].reshape(n, g_in.shape[2])
        for c in range(width // step):
            cut = slice(c * step, (c + 1) * step)
            premix[0:n, cut] = jnp.dot(g, wo[:, cut], preferred_element_type=F32)

        def norm(i, _):
            at = pl.multiple_of(i * 16, 16)
            x = premix[pl.ds(at, 16), :]
            scale = lax.rsqrt(jnp.mean(x * x, axis=-1, keepdims=True) + rms_eps)
            q = lo + lax.div(i, rows // 16)
            to = pl.multiple_of(lax.rem(i, rows // 16) * 16, 16)
            outv[q, pl.ds(to, 16), :] = (x * scale * pgain[...]).astype(BF16)
            return 0

        lax.fori_loop(0, n // 16, norm, 0, unroll=2)
        for q in range(lo, hi):
            pltpu.make_async_copy(outv.at[q], out.at[q], out_sem.at[q]).start()

    def scoped(name, function, *args):
        with jax.named_scope(name):
            function(*args)

    def over(lo, hi, function):
        def run(q, _):
            function(q)
            return 0

        lax.fori_loop(lo, hi, run, 0)

    def near(q):
        arrived(q, twin)
        project_kv(0, q, own_rows)
        project_qg(0, q, own_rows)

    def take(q):
        with jax.named_scope("take"):
            arrived(q, across)
        to_twin(q, False).start()

    def rest(q):
        with jax.named_scope("take2"):
            arrived(q, across_twin)
        project_kv(0, q, far_rows)
        project_qg(0, q, far_rows)

    scoped("near01", over, 0, 2, near)
    scoped("pass0", pass_on, 0)
    scoped("near23", over, 2, seqs, near)
    scoped("pass1", pass_on, 1)
    with jax.named_scope("tables1"):
        head_copy().wait_recv()
        tables(1)
    for load in loads[3:] + loads_o:
        load.wait()
    scoped("pass2", pass_on, 2)
    take(0)
    scoped("pass3", pass_on, 3)
    scoped("rest0", rest, 0)
    take(1)
    scoped("rest1", rest, 1)
    with jax.named_scope("havekv"):
        have(0)
        have(1)

    def early(q):
        project_kv(1, q, everything)
        make_state(q)

    scoped("early", over, 0, 2, early)

    def lone(q):
        project_kv(1, q, own_rows)

    scoped("lone", over, 2, seqs, lone)
    scoped("plane0", plane_total, 0)
    take(2)
    scoped("plane1", plane_total, 1)
    scoped("rest2", rest, 2)
    project_kv(1, 2, far_rows)
    scoped("state2", make_state, 2)
    with jax.named_scope("haveqg"):
        have(2)
        have(3)

    def later(q):
        project_qg(1, q, everything)

    scoped("later", over, 0, seqs - 1, later)
    project_qg(1, seqs - 1, own_rows)
    scoped("back0", hand_back, 0)
    end = seqs - 1
    take(end)
    scoped("plane2", plane_total, 2)
    with jax.named_scope("rest3"):
        arrived(end, across_twin)
        for h in range(2):
            project_kv(h, end, far_rows)
        make_state(end)
    scoped("back1", hand_back, 1)
    with jax.named_scope("qg3"):
        for h in range(2):
            project_qg(h, end, far_rows)
    scoped("back2", hand_back, 2)
    scoped("inside01", over, 0, 2, inside)
    scoped("plane3", plane_total, end)
    scoped("inside23", over, 2, seqs, inside)
    scoped("finish01", over, 0, 2, finish)
    scoped("back3", hand_back, end)
    scoped("finish2", over, 2, end, finish)
    scoped("emit0", emit, 0, end)
    scoped("finish3", finish, end)
    scoped("emit3", emit, end, seqs)

    def drain(q):
        to_across(q).wait_send()
        to_twin(q, True).wait_send()
        to_twin(q, False).wait_send()
        for j in range(NY):
            s1_copy(q, 1, j, True).wait_send()
            s3_copy(q, 1, j, True).wait_send()
            if j:
                s1_copy(q, 0, j, True).wait_send()
                s3_copy(q, 0, j, True).wait_send()
        for d in range(1, nz):
            @pl.when(z + d < nz)
            def _():
                s2_copy(q, d).wait_send()
        for u in (twin, across, across_twin):
            gated_copy(q, u, me).wait_send()

    with jax.named_scope("drain"):
        over(0, seqs, drain)
        for i in range(4):
            cross(i).wait_send()
            straight(i).wait_send()
            for j in range(1, NY):
                along(i, j, True).wait_send()
        head_copy().wait_send()
        for q in range(seqs):
            pltpu.make_async_copy(outv.at[q], out.at[q], out_sem.at[q]).wait()


def hand_over(source, out, held, in_sem, out_sem):
    pieces = range(source.shape[0])
    into = [pltpu.make_async_copy(source.at[i], held.at[i], in_sem.at[i]) for i in pieces]
    back = [pltpu.make_async_copy(held.at[i], out.at[i], out_sem.at[i]) for i in pieces]
    for copy in into:
        copy.start()
    for i in pieces:
        into[i].wait()
        back[i].start()
    for copy in back:
        copy.wait()


def solution(mesh):
    tp, sp = mesh.shape["tp"], mesh.shape["sp"]

    def body(tok, gain, wq, wk, wv, wg, decay, ngain, wo, pgain):
        seqs, rows, width = tok.shape
        length = rows * 4
        nz = sp // NY
        part = HEAD_DIM // NY
        half = HEAD_DIM // 2
        inv = np.float32(rope_base) ** (-np.arange(half, dtype=np.float32) / half)
        inv = jnp.asarray(np.concatenate([inv, inv])[None, :], F32)
        dma = pltpu.SemaphoreType.DMA
        hbm = pl.BlockSpec(memory_space=pltpu.HBM)
        vmem = pltpu.VMEM
        wide = vmem((2, seqs, length, HEAD_DIM), BF16)
        mixed = pl.pallas_call(
            functools.partial(kernel, tp, sp),
            out_shape=jax.ShapeDtypeStruct(tok.shape, BF16),
            in_specs=[
                hbm, hbm, hbm, hbm, hbm, hbm,
                pl.BlockSpec(memory_space=pltpu.SMEM), hbm, hbm, hbm, hbm,
            ],
            out_specs=hbm,
            scratch_shapes=[
                vmem((1, width), F32), vmem((1, width), F32), vmem((1, HEAD_DIM), F32),
                vmem((2, 8, HEAD_DIM), F32),
                vmem(tok.shape, BF16),
                vmem((seqs, length, width), BF16),
                vmem((2, width, 4 * HEAD_DIM), BF16),
                vmem(wo.shape, BF16),
                vmem((length, HEAD_DIM), F32), vmem((length, HEAD_DIM), F32),
                vmem((2, length, length), F32),
                vmem((2, length, HEAD_DIM), F32), vmem((2, length, HEAD_DIM), F32),
                wide, wide, wide, wide,
                vmem((2, seqs, length, HEAD_DIM), F32),
                vmem((2, seqs, length, HEAD_DIM), F32),
                vmem((2, seqs, HEAD_DIM, HEAD_DIM), BF16),
                vmem((seqs, 2 * NY, part, HEAD_DIM), BF16),
                vmem((seqs, part, HEAD_DIM), BF16),
                vmem((seqs, nz, part, HEAD_DIM), BF16),
                vmem((seqs, 2 * NY, part, HEAD_DIM), BF16),
                vmem((part, HEAD_DIM), F32),
                vmem((2, seqs, HEAD_DIM, HEAD_DIM), BF16),
                vmem((seqs, length, 2 * HEAD_DIM), BF16),
                vmem((seqs, rows, HEAD_DIM * tp), BF16),
                vmem((seqs * rows, width), F32),
                vmem(tok.shape, BF16),
                dma((seqs,)), dma((seqs, 2)), dma((seqs, 4)),
                dma((2, 4)), dma((2, 4)), dma((4, NY)), dma((4, NY)),
                dma(()), dma(()),
                dma((2, seqs, NY)), dma((seqs, 2 * NY)), dma((seqs, nz)), dma((seqs, nz)),
                dma((2, seqs, NY)), dma((2, seqs, NY)),
                dma((seqs, 4)), dma((seqs, 4)),
                dma((8,)), dma((8,)), dma((seqs,)), dma((seqs,)),
            ],
            compiler_params=pltpu.CompilerParams(
                collective_id=0, has_side_effects=True, vmem_limit_bytes=59 * 2**20
            ),
            name="retention",
        )(
            tok, gain[None, :], wq, wk, wv, wg, decay, ngain[None, :], wo, pgain[None, :], inv
        )
        return pl.pallas_call(
            hand_over,
            out_shape=jax.ShapeDtypeStruct(tok.shape, BF16),
            in_specs=[hbm],
            out_specs=hbm,
            scratch_shapes=[pltpu.VMEM(tok.shape, BF16), dma((seqs,)), dma((seqs,))],
            compiler_params=pltpu.CompilerParams(vmem_limit_bytes=59 * 2**20),
            name="hand_over",
        )(mixed)

    placed = (
        P(None, ("sp", "tp"), None),
        P(),
        P(None, "tp"),
        P(None, "tp"),
        P(None, "tp"),
        P(None, "tp"),
        P("tp"),
        P("tp"),
        P(),
        P(),
    )
    return jax.shard_map(
        body, mesh=mesh, in_specs=placed, out_specs=P(None, ("sp", "tp"), None), check_vma=False
    )
```

time: 76.3 us -> 75.1 us (0.984)
  Pallas kernels: 75.5 us -> 74.3 us
    pallas_call x1, Pallas kernels: 73.5 us -> 72.4 us  [body(): pl.pallas_call(functools.partial(kernel, tp, sp), out_shape=jax.ShapeDtyp...]
where the time goes in v2:
time: 75.1 us; the launch traced here: 75 us
  Pallas kernels  74.3 us (99%)
    pallas_call x1, Pallas kernels, body(): pl.pallas_call(functools.partial(kernel, tp, sp), out_shape=jax.ShapeDtyp...  72.4 us
    pallas_call x1, Pallas kernels, body(): pl.pallas_call(hand_over, out_shape=jax.ShapeDtypeStruct(tok.shape, BF16)...  1.98 us

profile of v2, /device:TPU:1, one launch (start us, length us, event | category | flops | bytes accessed | tf_op | source)
XLA Modules:
  0.0 75.0 jit_solution(7470208562901056859)
XLA Ops:
  0.7 72.4 %retention.1.source = bf16[4,64,2048]{2,1,0:T(8,128)(2,1)} custom-call(bf16[4,64,2048]{2,1,0:T(8,128)(2,1)} %tok.1, f32[1,2048]{1,0:T(1,128)} %bitcast.3, bf16[2048,128]{1,0:T(8,128)(2,1)} %wq_h.1, bf16[2048,128]{1,0:T(8,128)(2,1)} %wk_h.1, bf16[2048,128]{1,0:T(8,128)(2,1)} %wv_h.1, bf16[2048,128]{1,0:T(8,128)(2,1)} %wg_h.1, f32[1]{0:T(128)S(6)} %copy.12.decay, ...), custom_call_target="tpu_custom_call" | custom-call | tf_op jit(solution)/shard_map/retention/pallas_call | solution.py:525
  73.0 2.0 %hand_over.1 = bf16[4,64,2048]{2,1,0:T(8,128)(2,1)} custom-call(bf16[4,64,2048]{2,1,0:T(8,128)(2,1)} %retention.1.source), custom_call_target="tpu_custom_call" | custom-call | tf_op jit(solution)/shard_map/hand_over/pallas_call | solution.py:572

commit v3 on v2

--- a/solution.py
+++ b/solution.py
@@ -24,10 +24,10 @@
     tok, gain_h, wq_h, wk_h, wv_h, wg_h, decay, ngain_h, wo_h, pgain_h, inv_h,
     out,
     gain, pgain, inv, heads, tokv, gath, w, wo, cosv, sinv, mask, fade, reach,
-    qs, qr, ks, vs, sg, within, s1_out, s1_in, s2_out, s2_in, s3_out, carry, excl,
+    qs, qr, ks, vs, sg, within, s1_out, s1_in, s2_out, s2_in, s3_out, excl,
     g_out, g_in, premix, outv,
-    x_send, p_send, t_recv, wx_send, wx_recv, wy_send, wy_recv, h_send, h_recv,
-    s1_send, s1_recv, s2_send, s2_recv, s3_send, s3_recv, g_send, g_recv,
+    x_send, p_send, t_recv, w_send, wx_recv, h_recv,
+    s_send, s1_recv, s2_recv, s3_recv, g_send, g_recv,
     w_sem, o_sem, in_sem, out_sem,
 ):
     seqs, rows, width = tok.shape
@@ -70,11 +70,11 @@
     loads_o = [
         pltpu.make_async_copy(
             wo_h.at[pl.ds(pl.multiple_of(head_of(i // 2, i % 2) * HEAD_DIM, HEAD_DIM), HEAD_DIM), :],
-            wo.at[i * HEAD_DIM:(i + 1) * HEAD_DIM, :], o_sem.at[i],
+            wo.at[i * HEAD_DIM:(i + 1) * HEAD_DIM, :], o_sem,
         )
         for i in range(8)
     ]
-    for load in loads_w + loads_in + loads + loads_o:
+    for load in loads_in[:1] + loads[:3] + loads_in[1:] + loads_w + loads[3:] + loads_o:
         load.start()
 
     barrier = pltpu.get_barrier_semaphore()
@@ -97,52 +97,40 @@
     def cross(i):
         span = pl.ds(pl.multiple_of(direct + y * piece, 128), piece)
         return pltpu.make_async_remote_copy(
-            w.at[0, span, cuts[i]], w.at[1, span, cuts[i]], wx_send.at[0, i], wx_recv.at[0, i],
+            w.at[0, span, cuts[i]], w.at[1, span, cuts[i]], w_send, wx_recv.at[i],
             device_id={"tp": mirror}, device_id_type=MESH,
         )
 
     def straight(i):
         return pltpu.make_async_remote_copy(
             w.at[0, 0:direct, cuts[i]], w.at[1, 0:direct, cuts[i]],
-            wx_send.at[1, i], wx_recv.at[1, i],
+            w_send, wx_recv.at[4 + i // 2],
             device_id={"tp": mirror}, device_id_type=MESH,
         )
 
-    def along(i, j, mine):
+    def along(i, j):
         peer = lax.rem(y + j, NY)
-        owner = y if mine else peer
-        span = pl.ds(pl.multiple_of(direct + owner * piece, 128), piece)
-        return pltpu.make_async_remote_copy(
-            w.at[1, span, cuts[i]], w.at[1, span, cuts[i]], wy_send.at[i, j], wy_recv.at[i, owner],
+        span = pl.ds(pl.multiple_of(direct + y * piece, 128), piece)
+        return pltpu.make_async_remote_copy(
+            w.at[1, span, cuts[i]], w.at[1, span, cuts[i]], w_send, wx_recv.at[4 + i // 2],
             device_id={"sp": z * NY + peer}, device_id_type=MESH,
         )
 
     def pass_on(i):
         cross(i).wait_recv()
         for j in range(1, NY):
-            along(i, j, True).start()
-
-    def have(i):
-        straight(i).wait_recv()
-        for j in range(1, NY):
-            along(i, j, False).wait_recv()
+            along(i, j).start()
+
+    def have(k):
+        took = w.at[1, 0:width - piece, 256 * k:256 * (k + 1)]
+        pltpu.make_async_remote_copy(
+            took, took, w_send, wx_recv.at[4 + k], device_id={"tp": mirror}, device_id_type=MESH,
+        ).wait_recv()
 
     def head_copy():
         return pltpu.make_async_remote_copy(
-            heads.at[0], heads.at[1], h_send, h_recv, device_id={"tp": mirror}, device_id_type=MESH,
-        )
-
-    loads[0].wait()
-    heads[0, 0:1, :] = jnp.full((1, HEAD_DIM), decay[0], F32)
-    for load in loads_w:
-        load.wait()
-    with jax.named_scope("barrier"):
-        pl.semaphore_wait(barrier, 3 + NY - 1 + NY + nz - 1)
-    for i in range(4):
-        cross(i).start()
-    for i in range(4):
-        straight(i).start()
-    head_copy().start()
+            heads.at[0], heads.at[1], w_send, h_recv, device_id={"tp": mirror}, device_id_type=MESH,
+        )
 
     def block_copy(q, u, dest, sem):
         return pltpu.make_async_remote_copy(
@@ -151,13 +139,13 @@
         )
 
     def to_across(q):
-        return block_copy(q, me, across, x_send.at[q])
+        return block_copy(q, me, across, x_send)
 
     def to_twin(q, own):
-        return block_copy(q, me if own else across, twin, p_send.at[q, 0 if own else 1])
+        return block_copy(q, me if own else across, twin, p_send)
 
     def arrived(q, u):
-        block_copy(q, u, twin, x_send.at[q]).wait_recv()
+        block_copy(q, u, twin, x_send).wait_recv()
 
     def normalise(q):
         def norm(i, _):
@@ -175,13 +163,29 @@
         to_twin(q, True).start()
 
     with jax.named_scope("norm"):
+        loads[0].wait()
+        heads[0, 0:1, :] = jnp.full((1, HEAD_DIM), decay[0], F32)
         loads[1].wait()
-        for q in range(seqs):
+        for q in range(2):
             loads_in[q].wait()
             normalise(q)
-            if q > 0:
-                send(q - 1)
-        send(seqs - 1)
+    with jax.named_scope("barrier"):
+        pl.semaphore_wait(barrier, 3 + NY - 1 + NY + nz - 1)
+    send(0)
+    head_copy().start()
+    with jax.named_scope("norm2"):
+        loads_in[2].wait()
+        normalise(2)
+        send(1)
+        for i in range(4):
+            loads_w[i].wait()
+            cross(i).start()
+        for i in range(4):
+            straight(i).start()
+        loads_in[3].wait()
+        normalise(3)
+        send(2)
+        send(3)
 
     with jax.named_scope("tables"):
         loads[2].wait()
@@ -229,13 +233,12 @@
     def power(n):
         return jnp.exp(jnp.full((1, 1), decay[0] * n, F32))
 
-    def s1_copy(q, h, j, mine):
+    def s1_copy(q, h, j):
         peer = lax.rem(y + j, NY)
         dest = {"sp": z * NY + peer, "tp": mirror} if h else {"sp": z * NY + peer}
-        arrival = slot if mine else peer * 2 + (1 - group if h else group)
-        return pltpu.make_async_remote_copy(
-            s1_out.at[h, q, at_rows(peer, part), :], s1_in.at[q, arrival],
-            s1_send.at[h, q, j], s1_recv.at[q, arrival], device_id=dest, device_id_type=MESH,
+        return pltpu.make_async_remote_copy(
+            s1_out.at[h, q, at_rows(peer, part), :], s1_in.at[q, slot],
+            s_send.at[0], s1_recv.at[q], device_id=dest, device_id_type=MESH,
         )
 
     def make_state(q):
@@ -246,58 +249,56 @@
             )
             s1_out[h, q] = total.astype(BF16)
         for j in range(NY):
-            s1_copy(q, 1, j, True).start()
+            s1_copy(q, 1, j).start()
             if j:
-                s1_copy(q, 0, j, True).start()
+                s1_copy(q, 0, j).start()
         s1_in[q, slot] = s1_out[0, q, at_rows(y, part), :]
 
     def s2_copy(q, d):
         return pltpu.make_async_remote_copy(
-            s2_out.at[q], s2_in.at[q, d], s2_send.at[q, d], s2_recv.at[q, d],
+            s2_out.at[q], s2_in.at[q, d - 1], s_send.at[1], s2_recv.at[q],
             device_id={"sp": lax.rem(z + d, nz) * NY + y}, device_id_type=MESH,
         )
 
     def plane_total(q):
-        for j in range(NY):
-            s1_copy(q, 1, j, False).wait_recv()
-            if j:
-                s1_copy(q, 0, j, False).wait_recv()
+        took = s1_in.at[q, 0:2 * NY - 1]
+        pltpu.make_async_remote_copy(
+            took, took, s_send.at[0], s1_recv.at[q], device_id={"tp": mirror}, device_id_type=MESH,
+        ).wait_recv()
         step = power(length)
         total = s1_in[q, 0].astype(F32)
         for k in range(1, 2 * NY):
             total = total * step + s1_in[q, k].astype(F32)
         s2_out[q] = total.astype(BF16)
         for d in range(1, nz):
-            @pl.when(z + d < nz)
-            def _():
-                s2_copy(q, d).start()
-
-    def s3_copy(q, h, j, mine):
+            s2_copy(q, d).start()
+
+    def s3_copy(q, h, j):
         peer = lax.rem(y + j, NY)
         dest = {"sp": z * NY + peer, "tp": mirror} if h else {"sp": z * NY + peer}
-        owner = y if mine else peer
         return pltpu.make_async_remote_copy(
             s3_out.at[q, peer * 2 + (1 - group if h else group)],
-            excl.at[h, q, at_rows(owner, part), :],
-            s3_send.at[h, q, j], s3_recv.at[h, q, owner], device_id=dest, device_id_type=MESH,
+            excl.at[h, q, at_rows(y, part), :],
+            s_send.at[2], s3_recv.at[q], device_id=dest, device_id_type=MESH,
         )
 
     def hand_back(q):
-        carry[...] = jnp.zeros_like(carry)
+        pltpu.make_async_remote_copy(
+            s2_in.at[q], s2_in.at[q], s_send.at[1], s2_recv.at[q],
+            device_id={"tp": mirror}, device_id_type=MESH,
+        ).wait_recv()
+        before = jnp.zeros((part, HEAD_DIM), F32)
         for d in range(1, nz):
-            @pl.when(z >= d)
-            def _():
-                s2_copy(q, d).wait_recv()
-                carry[...] += power(line * NY * (d - 1)) * s2_in[q, d].astype(F32)
+            rate = power(line * NY * (d - 1)) * jnp.where(z >= d, 1.0, 0.0)
+            before = before + rate * s2_in[q, d - 1].astype(F32)
         step = power(length)
-        before = carry[...]
         for k in range(2 * NY):
             s3_out[q, k] = before.astype(BF16)
             before = before * step + s1_in[q, k].astype(F32)
         for j in range(NY):
-            s3_copy(q, 1, j, True).start()
+            s3_copy(q, 1, j).start()
             if j:
-                s3_copy(q, 0, j, True).start()
+                s3_copy(q, 0, j).start()
         excl[0, q, at_rows(y, part), :] = s3_out[q, slot]
 
     def inside(q):
@@ -316,15 +317,15 @@
     def gated_copy(q, dest, source):
         return pltpu.make_async_remote_copy(
             g_out.at[q, at_rows(dest, rows), :], g_in.at[q, :, at_rows(source, 2 * HEAD_DIM)],
-            g_send.at[q, dest], g_recv.at[q, source],
+            g_send, g_recv.at[q],
             device_id={"tp": base + dest}, device_id_type=MESH,
         )
 
     def finish(q):
-        for j in range(NY):
-            s3_copy(q, 1, j, False).wait_recv()
-            if j:
-                s3_copy(q, 0, j, False).wait_recv()
+        took = s1_in.at[q, 0:2 * NY - 1]
+        pltpu.make_async_remote_copy(
+            took, took, s_send.at[2], s3_recv.at[q], device_id={"tp": mirror}, device_id_type=MESH,
+        ).wait_recv()
         for k in range(2):
             here = at_rows((1 - side) if k == 0 else side, pair)
             for h in range(2):
@@ -343,8 +344,10 @@
                 g_in[q, :, at_rows(me, 2 * HEAD_DIM)] = g_out[q, at_rows(me, rows), :]
 
     def gated_wait(q):
-        for u in (twin, across, across_twin):
-            gated_copy(q, twin, u).wait_recv()
+        took = g_in.at[q, :, 0:6 * HEAD_DIM]
+        pltpu.make_async_remote_copy(
+            took, took, g_send, g_recv.at[q], device_id={"tp": mirror}, device_id_type=MESH,
+        ).wait_recv()
 
     def emit(lo, hi):
         n = (hi - lo) * rows
@@ -368,7 +371,7 @@
 
         lax.fori_loop(0, n // 16, norm, 0, unroll=2)
         for q in range(lo, hi):
-            pltpu.make_async_copy(outv.at[q], out.at[q], out_sem.at[q]).start()
+            pltpu.make_async_copy(outv.at[q], out.at[q], out_sem).start()
 
     def scoped(name, function, *args):
         with jax.named_scope(name):
@@ -397,6 +400,7 @@
         project_kv(0, q, far_rows)
         project_qg(0, q, far_rows)
 
+    end = seqs - 1
     scoped("near01", over, 0, 2, near)
     scoped("pass0", pass_on, 0)
     scoped("near23", over, 2, seqs, near)
@@ -404,8 +408,8 @@
     with jax.named_scope("tables1"):
         head_copy().wait_recv()
         tables(1)
-    for load in loads[3:] + loads_o:
-        load.wait()
+    loads[3].wait()
+    pltpu.make_async_copy(wo_h, wo, o_sem).wait()
     scoped("pass2", pass_on, 2)
     take(0)
     scoped("pass3", pass_on, 3)
@@ -414,84 +418,67 @@
     scoped("rest1", rest, 1)
     with jax.named_scope("havekv"):
         have(0)
-        have(1)
 
     def early(q):
         project_kv(1, q, everything)
         make_state(q)
 
-    scoped("early", over, 0, 2, early)
-
     def lone(q):
         project_kv(1, q, own_rows)
 
+    def later(q):
+        project_qg(1, q, everything)
+
+    scoped("early", over, 0, 2, early)
+    take(2)
     scoped("lone", over, 2, seqs, lone)
-    scoped("plane0", plane_total, 0)
-    take(2)
-    scoped("plane1", plane_total, 1)
     scoped("rest2", rest, 2)
     project_kv(1, 2, far_rows)
     scoped("state2", make_state, 2)
     with jax.named_scope("haveqg"):
-        have(2)
-        have(3)
-
-    def later(q):
-        project_qg(1, q, everything)
-
+        have(1)
     scoped("later", over, 0, seqs - 1, later)
-    project_qg(1, seqs - 1, own_rows)
-    scoped("back0", hand_back, 0)
-    end = seqs - 1
+    scoped("plane0", plane_total, 0)
+    scoped("plane1", plane_total, 1)
+    project_qg(1, end, own_rows)
     take(end)
-    scoped("plane2", plane_total, 2)
+    scoped("inside01", over, 0, 2, inside)
+    with jax.named_scope("take2e"):
+        arrived(end, across_twin)
     with jax.named_scope("rest3"):
-        arrived(end, across_twin)
         for h in range(2):
             project_kv(h, end, far_rows)
         make_state(end)
+    scoped("plane2", plane_total, 2)
+    scoped("back0", hand_back, 0)
     scoped("back1", hand_back, 1)
     with jax.named_scope("qg3"):
         for h in range(2):
             project_qg(h, end, far_rows)
+    scoped("inside23", over, 2, seqs, inside)
+    scoped("plane3", plane_total, end)
     scoped("back2", hand_back, 2)
-    scoped("inside01", over, 0, 2, inside)
-    scoped("plane3", plane_total, end)
-    scoped("inside23", over, 2, seqs, inside)
     scoped("finish01", over, 0, 2, finish)
     scoped("back3", hand_back, end)
-    scoped("finish2", over, 2, end, finish)
+    scoped("finish23", over, 2, seqs, finish)
     scoped("emit0", emit, 0, end)
-    scoped("finish3", finish, end)
     scoped("emit3", emit, end, seqs)
 
-    def drain(q):
-        to_across(q).wait_send()
-        to_twin(q, True).wait_send()
-        to_twin(q, False).wait_send()
-        for j in range(NY):
-            s1_copy(q, 1, j, True).wait_send()
-            s3_copy(q, 1, j, True).wait_send()
-            if j:
-                s1_copy(q, 0, j, True).wait_send()
-                s3_copy(q, 0, j, True).wait_send()
-        for d in range(1, nz):
-            @pl.when(z + d < nz)
-            def _():
-                s2_copy(q, d).wait_send()
-        for u in (twin, across, across_twin):
-            gated_copy(q, u, me).wait_send()
+    def sent(took, sem):
+        pltpu.make_async_remote_copy(
+            took, took, sem, h_recv, device_id={"tp": mirror}, device_id_type=MESH,
+        ).wait_send()
 
     with jax.named_scope("drain"):
-        over(0, seqs, drain)
-        for i in range(4):
-            cross(i).wait_send()
-            straight(i).wait_send()
-            for j in range(1, NY):
-                along(i, j, True).wait_send()
-        head_copy().wait_send()
-        for q in range(seqs):
-            pltpu.make_async_copy(outv.at[q], out.at[q], out_sem.at[q]).wait()
+        sent(tokv, x_send)
+        sent(gath.at[:, 0:2 * rows, :], p_send)
+        sent(w.at[0, :, :], w_send)
+        sent(heads.at[0], w_send)
+        sent(s1_in.at[:, 0:2 * NY - 1], s_send.at[0])
+        sent(s2_in, s_send.at[1])
+        sent(s3_out.at[:, 0:2 * NY - 1], s_send.at[2])
+        sent(g_in.at[:, :, 0:6 * HEAD_DIM], g_send)
+        pltpu.make_async_copy(outv, out, out_sem).wait()
 
 
 def hand_over(source, out, held, in_sem, out_sem):
@@ -546,21 +533,16 @@
                 vmem((2, seqs, HEAD_DIM, HEAD_DIM), BF16),
                 vmem((seqs, 2 * NY, part, HEAD_DIM), BF16),
                 vmem((seqs, part, HEAD_DIM), BF16),
-                vmem((seqs, nz, part, HEAD_DIM), BF16),
+                vmem((seqs, nz - 1, part, HEAD_DIM), BF16),
                 vmem((seqs, 2 * NY, part, HEAD_DIM), BF16),
-                vmem((part, HEAD_DIM), F32),
                 vmem((2, seqs, HEAD_DIM, HEAD_DIM), BF16),
                 vmem((seqs, length, 2 * HEAD_DIM), BF16),
                 vmem((seqs, rows, HEAD_DIM * tp), BF16),
                 vmem((seqs * rows, width), F32),
                 vmem(tok.shape, BF16),
-                dma((seqs,)), dma((seqs, 2)), dma((seqs, 4)),
-                dma((2, 4)), dma((2, 4)), dma((4, NY)), dma((4, NY)),
-                dma(()), dma(()),
-                dma((2, seqs, NY)), dma((seqs, 2 * NY)), dma((seqs, nz)), dma((seqs, nz)),
-                dma((2, seqs, NY)), dma((2, seqs, NY)),
-                dma((seqs, 4)), dma((seqs, 4)),
-                dma((8,)), dma((8,)), dma((seqs,)), dma((seqs,)),
+                dma(()), dma(()), dma((seqs, 4)), dma(()), dma((6,)), dma(()),
+                dma((3,)), dma((seqs,)), dma((seqs,)), dma((seqs,)), dma(()), dma((seqs,)),
+                dma((8,)), dma(()), dma((seqs,)), dma(()),
             ],
             compiler_params=pltpu.CompilerParams(
                 collective_id=0, has_side_effects=True, vmem_limit_bytes=59 * 2**20

time: 75.1 us -> 60.9 us (0.81)
  the two profiles are of different devices: /device:TPU:1 before, /device:TPU:3 now
where the time goes in v3:
time: 60.9 us; the launch traced here: 60.8 us
  Pallas kernels  60.1 us (99%)
  between operations  0.66 us (1%)
    pallas_call x1, Pallas kernels, body(): pl.pallas_call(functools.partial(kernel, tp, sp), out_shape=jax.ShapeDtyp...  58.2 us
    pallas_call x1, Pallas kernels, body(): pl.pallas_call(hand_over, out_shape=jax.ShapeDtypeStruct(tok.shape, BF16)...  1.98 us

profile of v3, /device:TPU:3, one launch (start us, length us, event | category | flops | bytes accessed | tf_op | source)
XLA Modules:
  0.0 60.8 jit_solution(15231425020212436754)
XLA Ops:
  0.7 58.2 %retention.1.source = bf16[4,64,2048]{2,1,0:T(8,128)(2,1)} custom-call(bf16[4,64,2048]{2,1,0:T(8,128)(2,1)} %tok.1, f32[1,2048]{1,0:T(1,128)} %bitcast.3, bf16[2048,128]{1,0:T(8,128)(2,1)} %wq_h.1, bf16[2048,128]{1,0:T(8,128)(2,1)} %wk_h.1, bf16[2048,128]{1,0:T(8,128)(2,1)} %wv_h.1, bf16[2048,128]{1,0:T(8,128)(2,1)} %wg_h.1, f32[1]{0:T(128)S(6)} %copy.12.decay, ...), custom_call_target="tpu_custom_call" | custom-call | tf_op jit(solution)/shard_map/retention/pallas_call | solution.py:512
  58.8 2.0 %hand_over.1 = bf16[4,64,2048]{2,1,0:T(8,128)(2,1)} custom-call(bf16[4,64,2048]{2,1,0:T(8,128)(2,1)} %retention.1.source), custom_call_target="tpu_custom_call" | custom-call | tf_op jit(solution)/shard_map/hand_over/pallas_call | solution.py:554

commit v4 on v3

--- a/solution.py
+++ b/solution.py
@@ -23,12 +23,12 @@
     tp, sp,
     tok, gain_h, wq_h, wk_h, wv_h, wg_h, decay, ngain_h, wo_h, pgain_h, inv_h,
     out,
-    gain, pgain, inv, heads, tokv, gath, w, wo, cosv, sinv, mask, fade, reach,
+    gain, pgain, inv, heads, tokv, raw, gath, w, wo, cosv, sinv, mask, fade, reach,
     qs, qr, ks, vs, sg, within, s1_out, s1_in, s2_out, s2_in, s3_out, excl,
-    g_out, g_in, premix, outv,
+    g_out, g_in, premix,
     x_send, p_send, t_recv, w_send, wx_recv, h_recv,
     s_send, s1_recv, s2_recv, s3_recv, g_send, g_recv,
-    w_sem, o_sem, in_sem, out_sem,
+    w_sem, o_sem, in_sem,
 ):
     seqs, rows, width = tok.shape
     pair = 2 * rows
@@ -50,7 +50,16 @@
     mirror = (3 - chip) * 2 + core
     slot = y * 2 + group
 
-    loads_in = [pltpu.make_async_copy(tok.at[q], tokv.at[q], in_sem.at[q]) for q in range(seqs)]
+    def at_rows(who, n):
+        return pl.ds(pl.multiple_of(who * n, n), n)
+
+    loads_in = [
+        pltpu.make_async_copy(
+            tok.at[q], tokv.at[q - 1] if q else raw.at[at_rows(me, rows), :], in_sem.at[q]
+        )
+        for q in range(seqs)
+    ]
+
     cuts = [slice(i * HEAD_DIM, (i + 1) * HEAD_DIM) for i in range(4)]
     loads_w = [
         pltpu.make_async_copy(a, w.at[0, :, cuts[i]], w_sem.at[i])
@@ -91,9 +100,6 @@
     for j in range(1, nz):
         greet({"sp": lax.rem(z + j, nz) * NY + y})
 
-    def at_rows(who, n):
-        return pl.ds(pl.multiple_of(who * n, n), n)
-
     def cross(i):
         span = pl.ds(pl.multiple_of(direct + y * piece, 128), piece)
         return pltpu.make_async_remote_copy(
@@ -133,59 +139,64 @@
         )
 
     def block_copy(q, u, dest, sem):
-        return pltpu.make_async_remote_copy(
-            gath.at[q, at_rows(u, rows), :], gath.at[q, at_rows(u, rows), :],
-            sem, t_recv.at[q, u], device_id={"tp": base + dest}, device_id_type=MESH,
-        )
-
-    def to_across(q):
-        return block_copy(q, me, across, x_send)
-
-    def to_twin(q, own):
-        return block_copy(q, me if own else across, twin, p_send)
+        held = raw.at[at_rows(u, rows), :] if q is None else gath.at[q, at_rows(u, rows), :]
+        return pltpu.make_async_remote_copy(
+            held, held, sem, t_recv.at[0 if q is None else q, u],
+            device_id={"tp": base + dest}, device_id_type=MESH,
+        )
+
+    def raw_own(dest, sem):
+        return pltpu.make_async_remote_copy(
+            tok.at[0], raw.at[at_rows(me, rows), :], sem, t_recv.at[0, me],
+            device_id={"tp": base + dest}, device_id_type=MESH,
+        )
 
     def arrived(q, u):
         block_copy(q, u, twin, x_send).wait_recv()
 
-    def normalise(q):
+    def normalise(source, q, u):
         def norm(i, _):
-            at = pl.multiple_of(i * 16, 16)
-            x = tokv[q, pl.ds(at, 16), :].astype(F32)
+            x = source(pl.multiple_of(i * 16, 16)).astype(F32)
             scale = lax.rsqrt(jnp.mean(x * x, axis=-1, keepdims=True) + rms_eps)
-            to = pl.ds(pl.multiple_of(me * rows + at, 16), 16)
+            to = pl.ds(pl.multiple_of(u * rows + i * 16, 16), 16)
             gath[q, to, :] = (x * scale * gain[...]).astype(BF16)
             return 0
 
         lax.fori_loop(0, rows // 16, norm, 0, unroll=2)
 
+    def norm_own(q):
+        loads_in[q].wait()
+        normalise(lambda at: tokv[q - 1, pl.ds(at, 16), :], q, me)
+
+    def norm_raw(u):
+        normalise(lambda at: raw[pl.ds(pl.multiple_of(u * rows + at, 16), 16), :], 0, u)
+
     def send(q):
-        to_across(q).start()
-        to_twin(q, True).start()
-
+        block_copy(q, me, across, x_send).start()
+        block_copy(q, me, twin, p_send).start()
+
+    with jax.named_scope("barrier"):
+        pl.semaphore_wait(barrier, 3 + NY - 1 + NY + nz - 1)
+    raw_own(across, x_send).start()
+    raw_own(twin, p_send).start()
     with jax.named_scope("norm"):
         loads[0].wait()
         heads[0, 0:1, :] = jnp.full((1, HEAD_DIM), decay[0], F32)
         loads[1].wait()
-        for q in range(2):
-            loads_in[q].wait()
-            normalise(q)
-    with jax.named_scope("barrier"):
-        pl.semaphore_wait(barrier, 3 + NY - 1 + NY + nz - 1)
-    send(0)
-    head_copy().start()
-    with jax.named_scope("norm2"):
-        loads_in[2].wait()
-        normalise(2)
+        norm_own(1)
+        head_copy().start()
+        norm_own(2)
         send(1)
         for i in range(4):
             loads_w[i].wait()
             cross(i).start()
         for i in range(4):
             straight(i).start()
-        loads_in[3].wait()
-        normalise(3)
+        norm_own(3)
         send(2)
         send(3)
+        loads_in[0].wait()
+        norm_raw(me)
 
     with jax.named_scope("tables"):
         loads[2].wait()
@@ -314,10 +325,10 @@
                     weight, vs[h, q, upto, :], preferred_element_type=F32
                 )
 
-    def gated_copy(q, dest, source):
+    def gated_copy(q, dest, source, near_by=0):
         return pltpu.make_async_remote_copy(
             g_out.at[q, at_rows(dest, rows), :], g_in.at[q, :, at_rows(source, 2 * HEAD_DIM)],
-            g_send, g_recv.at[q],
+            g_send, g_recv.at[near_by, q],
             device_id={"tp": base + dest}, device_id_type=MESH,
         )
 
@@ -340,38 +351,50 @@
                 gated_copy(q, across, me).start()
                 gated_copy(q, across_twin, me).start()
             else:
-                gated_copy(q, twin, me).start()
+                gated_copy(q, twin, me, 1).start()
                 g_in[q, :, at_rows(me, 2 * HEAD_DIM)] = g_out[q, at_rows(me, rows), :]
 
-    def gated_wait(q):
-        took = g_in.at[q, :, 0:6 * HEAD_DIM]
+    def gated_wait(q, near_by):
+        took = g_in.at[q, :, 0:(2 if near_by else 4) * HEAD_DIM]
         pltpu.make_async_remote_copy(
-            took, took, g_send, g_recv.at[q], device_id={"tp": mirror}, device_id_type=MESH,
+            took, took, g_send, g_recv.at[near_by, q],
+            device_id={"tp": mirror}, device_id_type=MESH,
         ).wait_recv()
 
-    def emit(lo, hi):
-        n = (hi - lo) * rows
-        with jax.named_scope("gated_wait"):
-            for q in range(lo, hi):
-                gated_wait(q)
-        step = 512
-        g = g_in[lo:hi].reshape(n, g_in.shape[2])
-        for c in range(width // step):
-            cut = slice(c * step, (c + 1) * step)
-            premix[0:n, cut] = jnp.dot(g, wo[:, cut], preferred_element_type=F32)
-
+    step = 512
+    side_cols = 4 * HEAD_DIM
+
+    def closing(lo, n):
         def norm(i, _):
             at = pl.multiple_of(i * 16, 16)
             x = premix[pl.ds(at, 16), :]
             scale = lax.rsqrt(jnp.mean(x * x, axis=-1, keepdims=True) + rms_eps)
             q = lo + lax.div(i, rows // 16)
             to = pl.multiple_of(lax.rem(i, rows // 16) * 16, 16)
-            outv[q, pl.ds(to, 16), :] = (x * scale * pgain[...]).astype(BF16)
+            out[q, pl.ds(to, 16), :] = (x * scale * pgain[...]).astype(BF16)
             return 0
 
         lax.fori_loop(0, n // 16, norm, 0, unroll=2)
-        for q in range(lo, hi):
-            pltpu.make_async_copy(outv.at[q], out.at[q], out_sem).start()
+
+    def emit(lo, hi):
+        n = (hi - lo) * rows
+        with jax.named_scope("gated_wait"):
+            for q in range(lo, hi):
+                gated_wait(q, 0)
+                gated_wait(q, 1)
+        g = g_in[lo:hi].reshape(n, g_in.shape[2])
+        for c in range(width // step):
+            cut = slice(c * step, (c + 1) * step)
+            premix[0:n, cut] = jnp.dot(g, wo[:, cut], preferred_element_type=F32)
+        closing(lo, n)
+
+    def emit_half(q, which, near_by):
+        gated_wait(q, near_by)
+        span = at_rows(which, side_cols)
+        for c in range(width // step):
+            cut = slice(c * step, (c + 1) * step)
+            term = jnp.dot(g_in[q, :, span], wo[span, cut], preferred_element_type=F32)
+            premix[0:rows, cut] = term if near_by else premix[0:rows, cut] + term
 
     def scoped(name, function, *args):
         with jax.named_scope(name):
@@ -389,10 +412,16 @@
         project_kv(0, q, own_rows)
         project_qg(0, q, own_rows)
 
+    def near_raw():
+        arrived(None, twin)
+        norm_raw(twin)
+        project_kv(0, 0, own_rows)
+        project_qg(0, 0, own_rows)
+
     def take(q):
         with jax.named_scope("take"):
             arrived(q, across)
-        to_twin(q, False).start()
+        block_copy(q, across, twin, p_send).start()
 
     def rest(q):
         with jax.named_scope("take2"):
@@ -400,10 +429,18 @@
         project_kv(0, q, far_rows)
         project_qg(0, q, far_rows)
 
+    def rest_raw():
+        norm_raw(across)
+        with jax.named_scope("take2"):
+            arrived(None, across_twin)
+        norm_raw(across_twin)
+        project_kv(0, 0, far_rows)
+        project_qg(0, 0, far_rows)
+
     end = seqs - 1
-    scoped("near01", over, 0, 2, near)
+    scoped("near0", near_raw)
     scoped("pass0", pass_on, 0)
-    scoped("near23", over, 2, seqs, near)
+    scoped("near123", over, 1, seqs, near)
     scoped("pass1", pass_on, 1)
     with jax.named_scope("tables1"):
         head_copy().wait_recv()
@@ -411,9 +448,9 @@
     loads[3].wait()
     pltpu.make_async_copy(wo_h, wo, o_sem).wait()
     scoped("pass2", pass_on, 2)
-    take(0)
+    take(None)
     scoped("pass3", pass_on, 3)
-    scoped("rest0", rest, 0)
+    scoped("rest0", rest_raw)
     take(1)
     scoped("rest1", rest, 1)
     with jax.named_scope("havekv"):
@@ -450,19 +487,21 @@
             project_kv(h, end, far_rows)
         make_state(end)
     scoped("plane2", plane_total, 2)
-    scoped("back0", hand_back, 0)
-    scoped("back1", hand_back, 1)
     with jax.named_scope("qg3"):
         for h in range(2):
             project_qg(h, end, far_rows)
     scoped("inside23", over, 2, seqs, inside)
+    scoped("back0", hand_back, 0)
+    scoped("back1", hand_back, 1)
     scoped("plane3", plane_total, end)
     scoped("back2", hand_back, 2)
     scoped("finish01", over, 0, 2, finish)
     scoped("back3", hand_back, end)
     scoped("finish23", over, 2, seqs, finish)
     scoped("emit0", emit, 0, end)
-    scoped("emit3", emit, end, seqs)
+    scoped("emit3a", emit_half, end, side, 1)
+    scoped("emit3b", emit_half, end, 1 - side, 0)
+    scoped("closing", closing, end, rows)
 
     def sent(took, sem):
         pltpu.make_async_remote_copy(
@@ -470,7 +509,7 @@
         ).wait_send()
 
     with jax.named_scope("drain"):
-        sent(tokv, x_send)
+        sent(gath.at[:, 0:rows, :], x_send)
         sent(gath.at[:, 0:2 * rows, :], p_send)
         sent(w.at[0, :, :], w_send)
         sent(heads.at[0], w_send)
@@ -478,20 +517,12 @@
         sent(s2_in, s_send.at[1])
         sent(s3_out.at[:, 0:2 * NY - 1], s_send.at[2])
         sent(g_in.at[:, :, 0:6 * HEAD_DIM], g_send)
-        pltpu.make_async_copy(outv, out, out_sem).wait()
-
-
-def hand_over(source, out, held, in_sem, out_sem):
-    pieces = range(source.shape[0])
-    into = [pltpu.make_async_copy(source.at[i], held.at[i], in_sem.at[i]) for i in pieces]
-    back = [pltpu.make_async_copy(held.at[i], out.at[i], out_sem.at[i]) for i in pieces]
-    for copy in into:
-        copy.start()
-    for i in pieces:
-        into[i].wait()
-        back[i].start()
-    for copy in back:
-        copy.wait()
+
+
+def hand_over(source, out, sem):
+    copy = pltpu.make_async_copy(source, out, sem)
+    copy.start()
+    copy.wait()
 
 
 def solution(mesh):
@@ -516,11 +547,12 @@
                 hbm, hbm, hbm, hbm, hbm, hbm,
                 pl.BlockSpec(memory_space=pltpu.SMEM), hbm, hbm, hbm, hbm,
             ],
-            out_specs=hbm,
+            out_specs=pl.BlockSpec(memory_space=pltpu.VMEM),
             scratch_shapes=[
                 vmem((1, width), F32), vmem((1, width), F32), vmem((1, HEAD_DIM), F32),
                 vmem((2, 8, HEAD_DIM), F32),
-                vmem(tok.shape, BF16),
+                vmem((seqs - 1, rows, width), BF16),
+                vmem((length, width), BF16),
                 vmem((seqs, length, width), BF16),
                 vmem((2, width, 4 * HEAD_DIM), BF16),
                 vmem(wo.shape, BF16),
@@ -539,25 +571,25 @@
                 vmem((seqs, length, 2 * HEAD_DIM), BF16),
                 vmem((seqs, rows, HEAD_DIM * tp), BF16),
                 vmem((seqs * rows, width), F32),
-                vmem(tok.shape, BF16),
                 dma(()), dma(()), dma((seqs, 4)), dma(()), dma((6,)), dma(()),
-                dma((3,)), dma((seqs,)), dma((seqs,)), dma((seqs,)), dma(()), dma((seqs,)),
-                dma((8,)), dma(()), dma((seqs,)), dma(()),
+                dma((3,)), dma((seqs,)), dma((seqs,)), dma((seqs,)), dma(()), dma((2, seqs)),
+                dma((8,)), dma(()), dma((seqs,)),
             ],
             compiler_params=pltpu.CompilerParams(
-                collective_id=0, has_side_effects=True, vmem_limit_bytes=59 * 2**20
+                collective_id=0, has_side_effects=True, vmem_limit_bytes=40 * 2**20
             ),
             name="retention",
         )(
-            tok, gain[None, :], wq, wk, wv, wg, decay, ngain[None, :], wo, pgain[None, :], inv
+            *(pltpu.with_memory_space_constraint(x, pltpu.HBM) for x in (tok, gain[None, :], wq, wk, wv, wg)), decay,
+            *(pltpu.with_memory_space_constraint(x, pltpu.HBM) for x in (ngain[None, :], wo, pgain[None, :], inv))
         )
         return pl.pallas_call(
             hand_over,
             out_shape=jax.ShapeDtypeStruct(tok.shape, BF16),
-            in_specs=[hbm],
+            in_specs=[pl.BlockSpec(memory_space=pltpu.VMEM)],
             out_specs=hbm,
-            scratch_shapes=[pltpu.VMEM(tok.shape, BF16), dma((seqs,)), dma((seqs,))],
-            compiler_params=pltpu.CompilerParams(vmem_limit_bytes=59 * 2**20),
+            scratch_shapes=[dma(())],
+            compiler_params=pltpu.CompilerParams(vmem_limit_bytes=16 * 2**20),
             name="hand_over",
         )(mixed)
 

time: 60.9 us -> 58.7 us (0.964)
  the two profiles are of different devices: /device:TPU:3 before, /device:TPU:1 now
where the time goes in v4:
time: 58.7 us
  Pallas kernels  58 us (99%)
  between operations  0.66 us (1%)
    pallas_call x1, Pallas kernels, body(): pl.pallas_call(functools.partial(kernel, tp, sp), out_shape=jax.ShapeDtyp...  57 us

profile of v4, /device:TPU:1, one launch (start us, length us, event | category | flops | bytes accessed | tf_op | source)
XLA Modules:
  0.0 58.7 jit_solution(18317386831973673584)
XLA Ops:
  0.7 57.0 %retention.1.source = bf16[4,64,2048]{2,1,0:T(8,128)(2,1)S(1)} custom-call(bf16[4,64,2048]{2,1,0:T(8,128)(2,1)} %tok.1, f32[1,2048]{1,0:T(1,128)} %bitcast.3, bf16[2048,128]{1,0:T(8,128)(2,1)} %wq_h.1, bf16[2048,128]{1,0:T(8,128)(2,1)} %wk_h.1, bf16[2048,128]{1,0:T(8,128)(2,1)} %wv_h.1, bf16[2048,128]{1,0:T(8,128)(2,1)} %wg_h.1, f32[1]{0:T(128)S(6)} %copy.12.decay, ...), custom_call_target="tpu_custom_call" | custom-call | tf_op jit(solution)/shard_map/retention/pallas_call | solution.py:543
  57.7 1.0 %hand_over.1 = bf16[4,64,2048]{2,1,0:T(8,128)(2,1)} custom-call(bf16[4,64,2048]{2,1,0:T(8,128)(2,1)S(1)} %retention.1.source), custom_call_target="tpu_custom_call" | custom-call | tf_op jit(solution)/shard_map/hand_over/pallas_call | solution.py:586

commit v5 on v4

--- a/solution.py
+++ b/solution.py
@@ -28,7 +28,7 @@
     g_out, g_in, premix,
     x_send, p_send, t_recv, w_send, wx_recv, h_recv,
     s_send, s1_recv, s2_recv, s3_recv, g_send, g_recv,
-    w_sem, o_sem, in_sem,
+    w_sem, o_sem, in_sem, present,
 ):
     seqs, rows, width = tok.shape
     pair = 2 * rows
@@ -97,8 +97,10 @@
         greet({"sp": z * NY + lax.rem(y + j, NY)})
     for j in range(NY):
         greet({"sp": z * NY + lax.rem(y + j, NY), "tp": mirror})
-    for j in range(1, nz):
-        greet({"sp": lax.rem(z + j, nz) * NY + y})
+    for d in range(1, nz):
+        @pl.when(z + d < nz)
+        def _():
+            greet({"sp": lax.rem(z + d, nz) * NY + y})
 
     def cross(i):
         span = pl.ds(pl.multiple_of(direct + y * piece, 128), piece)
@@ -176,9 +178,16 @@
         block_copy(q, me, twin, p_send).start()
 
     with jax.named_scope("barrier"):
-        pl.semaphore_wait(barrier, 3 + NY - 1 + NY + nz - 1)
+        pl.semaphore_wait(barrier, 3 + NY - 1 + NY + z)
     raw_own(across, x_send).start()
     raw_own(twin, p_send).start()
+    for d in range(1, nz):
+        @pl.when(z >= d)
+        def _():
+            pl.semaphore_signal(
+                present, inc=1, device_id={"sp": lax.rem(z + nz - d, nz) * NY + y},
+                device_id_type=MESH,
+            )
     with jax.named_scope("norm"):
         loads[0].wait()
         heads[0, 0:1, :] = jnp.full((1, HEAD_DIM), decay[0], F32)
@@ -282,7 +291,9 @@
             total = total * step + s1_in[q, k].astype(F32)
         s2_out[q] = total.astype(BF16)
         for d in range(1, nz):
-            s2_copy(q, d).start()
+            @pl.when(z + d < nz)
+            def _():
+                s2_copy(q, d).start()
 
     def s3_copy(q, h, j):
         peer = lax.rem(y + j, NY)
@@ -294,14 +305,19 @@
         )
 
     def hand_back(q):
-        pltpu.make_async_remote_copy(
-            s2_in.at[q], s2_in.at[q], s_send.at[1], s2_recv.at[q],
-            device_id={"tp": mirror}, device_id_type=MESH,
-        ).wait_recv()
-        before = jnp.zeros((part, HEAD_DIM), F32)
-        for d in range(1, nz):
-            rate = power(line * NY * (d - 1)) * jnp.where(z >= d, 1.0, 0.0)
-            before = before + rate * s2_in[q, d - 1].astype(F32)
+        for n in range(1, nz):
+            @pl.when(z == n)
+            def _():
+                took = s2_in.at[q, 0:n]
+                pltpu.make_async_remote_copy(
+                    took, took, s_send.at[1], s2_recv.at[q],
+                    device_id={"tp": mirror}, device_id_type=MESH,
+                ).wait_recv()
+
+        def add(d, total):
+            return total + power(line * NY * d) * s2_in[q, d].astype(F32)
+
+        before = lax.fori_loop(0, z, add, jnp.zeros((part, HEAD_DIM), F32))
         step = power(length)
         for k in range(2 * NY):
             s3_out[q, k] = before.astype(BF16)
@@ -474,12 +490,17 @@
     scoped("state2", make_state, 2)
     with jax.named_scope("haveqg"):
         have(1)
-    scoped("later", over, 0, seqs - 1, later)
+    scoped("later01", over, 0, 2, later)
+    with jax.named_scope("present"):
+        @pl.when(z < nz - 1)
+        def _():
+            pl.semaphore_wait(present, nz - 1 - z)
+
     scoped("plane0", plane_total, 0)
     scoped("plane1", plane_total, 1)
+    take(end)
+    scoped("later2", later, 2)
     project_qg(1, end, own_rows)
-    take(end)
-    scoped("inside01", over, 0, 2, inside)
     with jax.named_scope("take2e"):
         arrived(end, across_twin)
     with jax.named_scope("rest3"):
@@ -490,10 +511,12 @@
     with jax.named_scope("qg3"):
         for h in range(2):
             project_qg(h, end, far_rows)
-    scoped("inside23", over, 2, seqs, inside)
+    scoped("inside01", over, 0, 2, inside)
     scoped("back0", hand_back, 0)
     scoped("back1", hand_back, 1)
+    scoped("inside2", inside, 2)
     scoped("plane3", plane_total, end)
+    scoped("inside3", inside, end)
     scoped("back2", hand_back, 2)
     scoped("finish01", over, 0, 2, finish)
     scoped("back3", hand_back, end)
@@ -514,7 +537,10 @@
         sent(w.at[0, :, :], w_send)
         sent(heads.at[0], w_send)
         sent(s1_in.at[:, 0:2 * NY - 1], s_send.at[0])
-        sent(s2_in, s_send.at[1])
+        for n in range(nz - 1):
+            @pl.when(z == n)
+            def _():
+                sent(s2_in.at[:, 0:nz - 1 - n], s_send.at[1])
         sent(s3_out.at[:, 0:2 * NY - 1], s_send.at[2])
         sent(g_in.at[:, :, 0:6 * HEAD_DIM], g_send)
 
@@ -573,7 +599,7 @@
                 vmem((seqs * rows, width), F32),
                 dma(()), dma(()), dma((seqs, 4)), dma(()), dma((6,)), dma(()),
                 dma((3,)), dma((seqs,)), dma((seqs,)), dma((seqs,)), dma(()), dma((2, seqs)),
-                dma((8,)), dma(()), dma((seqs,)),
+                dma((8,)), dma(()), dma((seqs,)), pltpu.SemaphoreType.REGULAR,
             ],
             compiler_params=pltpu.CompilerParams(
                 collective_id=0, has_side_effects=True, vmem_limit_bytes=40 * 2**20

time: 58.7 us -> 52.2 us (0.89)
  the two profiles are of different devices: /device:TPU:1 before, /device:TPU:227 now
where the time goes in v5:
time: 52.2 us; the launch traced here: 52.1 us
  Pallas kernels  51.5 us (99%)
  between operations  0.66 us (1%)
    pallas_call x1, Pallas kernels, body(): pl.pallas_call(functools.partial(kernel, tp, sp), out_shape=jax.ShapeDtyp...  50.5 us

profile of v5, /device:TPU:227, one launch (start us, length us, event | category | flops | bytes accessed | tf_op | source)
XLA Modules:
  0.0 52.1 jit_solution(860247357987437031)
XLA Ops:
  0.7 50.5 %retention.1.source = bf16[4,64,2048]{2,1,0:T(8,128)(2,1)S(1)} custom-call(bf16[4,64,2048]{2,1,0:T(8,128)(2,1)} %tok.1, f32[1,2048]{1,0:T(1,128)} %bitcast.3, bf16[2048,128]{1,0:T(8,128)(2,1)} %wq_h.1, bf16[2048,128]{1,0:T(8,128)(2,1)} %wk_h.1, bf16[2048,128]{1,0:T(8,128)(2,1)} %wv_h.1, bf16[2048,128]{1,0:T(8,128)(2,1)} %wg_h.1, f32[1]{0:T(128)S(6)} %copy.12.decay, ...), custom_call_target="tpu_custom_call" | custom-call | tf_op jit(solution)/shard_map/retention/pallas_call | solution.py:569
  51.1 1.0 %hand_over.1 = bf16[4,64,2048]{2,1,0:T(8,128)(2,1)} custom-call(bf16[4,64,2048]{2,1,0:T(8,128)(2,1)S(1)} %retention.1.source), custom_call_target="tpu_custom_call" | custom-call | tf_op jit(solution)/shard_map/hand_over/pallas_call | solution.py:612

commit v6 on v5

--- a/solution.py
+++ b/solution.py
@@ -26,7 +26,7 @@
     gain, pgain, inv, heads, tokv, raw, gath, w, wo, cosv, sinv, mask, fade, reach,
     qs, qr, ks, vs, sg, within, s1_out, s1_in, s2_out, s2_in, s3_out, excl,
     g_out, g_in, premix,
-    x_send, p_send, t_recv, w_send, wx_recv, h_recv,
+    x_send, p_send, t_recv, last_recv, w_send, wx_recv, h_recv,
     s_send, s1_recv, s2_recv, s3_recv, g_send, g_recv,
     w_sem, o_sem, in_sem, present,
 ):
@@ -83,7 +83,7 @@
         )
         for i in range(8)
     ]
-    for load in loads_in[:1] + loads[:3] + loads_in[1:] + loads_w + loads[3:] + loads_o:
+    for load in loads_in + loads:
         load.start()
 
     barrier = pltpu.get_barrier_semaphore()
@@ -147,12 +147,6 @@
             device_id={"tp": base + dest}, device_id_type=MESH,
         )
 
-    def raw_own(dest, sem):
-        return pltpu.make_async_remote_copy(
-            tok.at[0], raw.at[at_rows(me, rows), :], sem, t_recv.at[0, me],
-            device_id={"tp": base + dest}, device_id_type=MESH,
-        )
-
     def arrived(q, u):
         block_copy(q, u, twin, x_send).wait_recv()
 
@@ -177,10 +171,27 @@
         block_copy(q, me, across, x_send).start()
         block_copy(q, me, twin, p_send).start()
 
+    def last_copy(u, late, dest, sem, arrival):
+        span = pl.ds(pl.multiple_of(u * rows + late * (rows - 16), 16), 16 if late else rows - 16)
+        held = gath.at[seqs - 1, span, :]
+        return pltpu.make_async_remote_copy(
+            held, held, sem, arrival, device_id={"tp": base + dest}, device_id_type=MESH,
+        )
+
+    def take_last():
+        for late in range(2):
+            with jax.named_scope("takelast"):
+                last_copy(across, late, twin, p_send, last_recv.at[late]).wait_recv()
+            last_copy(across, late, twin, p_send, t_recv.at[seqs - 1, across]).start()
+
+    with jax.named_scope("load0"):
+        loads_in[0].wait()
+    for load in loads_w:
+        load.start()
     with jax.named_scope("barrier"):
         pl.semaphore_wait(barrier, 3 + NY - 1 + NY + z)
-    raw_own(across, x_send).start()
-    raw_own(twin, p_send).start()
+    block_copy(None, me, across, x_send).start()
+    block_copy(None, me, twin, p_send).start()
     for d in range(1, nz):
         @pl.when(z >= d)
         def _():
@@ -201,10 +212,13 @@
             cross(i).start()
         for i in range(4):
             straight(i).start()
+        for load in loads_o:
+            load.start()
         norm_own(3)
         send(2)
-        send(3)
-        loads_in[0].wait()
+        for late in range(2):
+            last_copy(me, late, across, x_send, last_recv.at[late]).start()
+        block_copy(seqs - 1, me, twin, p_send).start()
         norm_raw(me)
 
     with jax.named_scope("tables"):
@@ -404,13 +418,16 @@
             premix[0:n, cut] = jnp.dot(g, wo[:, cut], preferred_element_type=F32)
         closing(lo, n)
 
-    def emit_half(q, which, near_by):
-        gated_wait(q, near_by)
+    def emit_half(lo, hi, which, near_by):
+        for q in range(lo, hi):
+            gated_wait(q, near_by)
+        n = (hi - lo) * rows
         span = at_rows(which, side_cols)
+        g = g_in[lo:hi, :, span].reshape(n, side_cols)
         for c in range(width // step):
             cut = slice(c * step, (c + 1) * step)
-            term = jnp.dot(g_in[q, :, span], wo[span, cut], preferred_element_type=F32)
-            premix[0:rows, cut] = term if near_by else premix[0:rows, cut] + term
+            term = jnp.dot(g, wo[span, cut], preferred_element_type=F32)
+            premix[0:n, cut] = term if near_by else premix[0:n, cut] + term
 
     def scoped(name, function, *args):
         with jax.named_scope(name):
@@ -490,17 +507,16 @@
     scoped("state2", make_state, 2)
     with jax.named_scope("haveqg"):
         have(1)
-    scoped("later01", over, 0, 2, later)
+    take_last()
+    scoped("later0", over, 0, 1, later)
     with jax.named_scope("present"):
         @pl.when(z < nz - 1)
         def _():
             pl.semaphore_wait(present, nz - 1 - z)
 
     scoped("plane0", plane_total, 0)
+    project_qg(1, end, own_rows)
     scoped("plane1", plane_total, 1)
-    take(end)
-    scoped("later2", later, 2)
-    project_qg(1, end, own_rows)
     with jax.named_scope("take2e"):
         arrived(end, across_twin)
     with jax.named_scope("rest3"):
@@ -511,19 +527,20 @@
     with jax.named_scope("qg3"):
         for h in range(2):
             project_qg(h, end, far_rows)
-    scoped("inside01", over, 0, 2, inside)
+    scoped("later12", over, 1, seqs - 1, later)
     scoped("back0", hand_back, 0)
     scoped("back1", hand_back, 1)
-    scoped("inside2", inside, 2)
+    scoped("inside01", over, 0, 2, inside)
     scoped("plane3", plane_total, end)
-    scoped("inside3", inside, end)
     scoped("back2", hand_back, 2)
+    scoped("inside23", over, 2, seqs, inside)
+    scoped("back3", hand_back, end)
     scoped("finish01", over, 0, 2, finish)
-    scoped("back3", hand_back, end)
     scoped("finish23", over, 2, seqs, finish)
-    scoped("emit0", emit, 0, end)
-    scoped("emit3a", emit_half, end, side, 1)
-    scoped("emit3b", emit_half, end, 1 - side, 0)
+    scoped("emit0", emit, 0, 2)
+    scoped("emit2", emit, 2, end)
+    scoped("emit3a", emit_half, end, seqs, side, 1)
+    scoped("emit3b", emit_half, end, seqs, 1 - side, 0)
     scoped("closing", closing, end, rows)
 
     def sent(took, sem):
@@ -597,7 +614,7 @@
                 vmem((seqs, length, 2 * HEAD_DIM), BF16),
                 vmem((seqs, rows, HEAD_DIM * tp), BF16),
                 vmem((seqs * rows, width), F32),
-                dma(()), dma(()), dma((seqs, 4)), dma(()), dma((6,)), dma(()),
+                dma(()), dma(()), dma((seqs, 4)), dma((2,)), dma(()), dma((6,)), dma(()),
                 dma((3,)), dma((seqs,)), dma((seqs,)), dma((seqs,)), dma(()), dma((2, seqs)),
                 dma((8,)), dma(()), dma((seqs,)), pltpu.SemaphoreType.REGULAR,
             ],

time: 52.2 us -> 50.9 us (0.975)
  Pallas kernels: 51.5 us -> 50.1 us
    pallas_call x1, Pallas kernels: 50.5 us -> 49.1 us  [body(): pl.pallas_call(functools.partial(kernel, tp, sp), out_shape=jax.ShapeDtyp...]
where the time goes in v6:
time: 50.9 us; the launch traced here: 50.8 us
  Pallas kernels  50.1 us (98%)
  between operations  0.66 us (1%)
    pallas_call x1, Pallas kernels, body(): pl.pallas_call(functools.partial(kernel, tp, sp), out_shape=jax.ShapeDtyp...  49.1 us

profile of v6, /device:TPU:227, one launch (start us, length us, event | category | flops | bytes accessed | tf_op | source)
XLA Modules:
  0.0 50.8 jit_solution(18232622000965715472)
XLA Ops:
  0.7 49.1 %retention.1.source = bf16[4,64,2048]{2,1,0:T(8,128)(2,1)S(1)} custom-call(bf16[4,64,2048]{2,1,0:T(8,128)(2,1)} %tok.1, f32[1,2048]{1,0:T(1,128)} %bitcast.3, bf16[2048,128]{1,0:T(8,128)(2,1)} %wq_h.1, bf16[2048,128]{1,0:T(8,128)(2,1)} %wk_h.1, bf16[2048,128]{1,0:T(8,128)(2,1)} %wv_h.1, bf16[2048,128]{1,0:T(8,128)(2,1)} %wg_h.1, f32[1]{0:T(128)S(6)} %copy.12.decay, ...), custom_call_target="tpu_custom_call" | custom-call | tf_op jit(solution)/shard_map/retention/pallas_call | solution.py:586
  49.8 1.0 %hand_over.1 = bf16[4,64,2048]{2,1,0:T(8,128)(2,1)} custom-call(bf16[4,64,2048]{2,1,0:T(8,128)(2,1)S(1)} %retention.1.source), custom_call_target="tpu_custom_call" | custom-call | tf_op jit(solution)/shard_map/hand_over/pallas_call | solution.py:629

commit v7 on v6

--- a/solution.py
+++ b/solution.py
@@ -22,10 +22,10 @@
 def kernel(
     tp, sp,
     tok, gain_h, wq_h, wk_h, wv_h, wg_h, decay, ngain_h, wo_h, pgain_h, inv_h,
-    out,
-    gain, pgain, inv, heads, tokv, raw, gath, w, wo, cosv, sinv, mask, fade, reach,
+    out, premix, pgain,
+    gain, inv, heads, tokv, raw, gath, w, wo, cosv, sinv, mask, fade, reach,
     qs, qr, ks, vs, sg, within, s1_out, s1_in, s2_out, s2_in, s3_out, excl,
-    g_out, g_in, premix,
+    g_out, g_in,
     x_send, p_send, t_recv, last_recv, w_send, wx_recv, h_recv,
     s_send, s1_recv, s2_recv, s3_recv, g_send, g_recv,
     w_sem, o_sem, in_sem, present,
@@ -215,11 +215,11 @@
         for load in loads_o:
             load.start()
         norm_own(3)
+        norm_raw(me)
         send(2)
         for late in range(2):
             last_copy(me, late, across, x_send, last_recv.at[late]).start()
         block_copy(seqs - 1, me, twin, p_send).start()
-        norm_raw(me)
 
     with jax.named_scope("tables"):
         loads[2].wait()
@@ -537,11 +537,9 @@
     scoped("back3", hand_back, end)
     scoped("finish01", over, 0, 2, finish)
     scoped("finish23", over, 2, seqs, finish)
-    scoped("emit0", emit, 0, 2)
-    scoped("emit2", emit, 2, end)
+    scoped("emit0", emit, 0, end)
     scoped("emit3a", emit_half, end, seqs, side, 1)
     scoped("emit3b", emit_half, end, seqs, 1 - side, 0)
-    scoped("closing", closing, end, rows)
 
     def sent(took, sem):
         pltpu.make_async_remote_copy(
@@ -562,10 +560,23 @@
         sent(g_in.at[:, :, 0:6 * HEAD_DIM], g_send)
 
 
-def hand_over(source, out, sem):
-    copy = pltpu.make_async_copy(source, out, sem)
-    copy.start()
-    copy.wait()
+def hand_over(source, premix, pgain, out, held, sem):
+    seqs, rows, _ = source.shape
+    done = pltpu.make_async_copy(source.at[0:seqs - 1], out.at[0:seqs - 1], sem.at[0])
+    done.start()
+
+    def norm(i, _):
+        at = pl.multiple_of(i * 16, 16)
+        x = premix[pl.ds(at, 16), :]
+        scale = lax.rsqrt(jnp.mean(x * x, axis=-1, keepdims=True) + rms_eps)
+        held[pl.ds(at, 16), :] = (x * scale * pgain[...]).astype(BF16)
+        return 0
+
+    lax.fori_loop(0, rows // 16, norm, 0, unroll=2)
+    last = pltpu.make_async_copy(held, out.at[seqs - 1], sem.at[1])
+    last.start()
+    done.wait()
+    last.wait()
 
 
 def solution(mesh):
@@ -583,16 +594,20 @@
         hbm = pl.BlockSpec(memory_space=pltpu.HBM)
         vmem = pltpu.VMEM
         wide = vmem((2, seqs, length, HEAD_DIM), BF16)
-        mixed = pl.pallas_call(
+        mixed, premix, post = pl.pallas_call(
             functools.partial(kernel, tp, sp),
-            out_shape=jax.ShapeDtypeStruct(tok.shape, BF16),
+            out_shape=(
+                jax.ShapeDtypeStruct(tok.shape, BF16),
+                jax.ShapeDtypeStruct((seqs * rows, width), F32),
+                jax.ShapeDtypeStruct((1, width), F32),
+            ),
             in_specs=[
                 hbm, hbm, hbm, hbm, hbm, hbm,
                 pl.BlockSpec(memory_space=pltpu.SMEM), hbm, hbm, hbm, hbm,
             ],
-            out_specs=pl.BlockSpec(memory_space=pltpu.VMEM),
+            out_specs=(pl.BlockSpec(memory_space=pltpu.VMEM),) * 3,
             scratch_shapes=[
-                vmem((1, width), F32), vmem((1, width), F32), vmem((1, HEAD_DIM), F32),
+                vmem((1, width), F32), vmem((1, HEAD_DIM), F32),
                 vmem((2, 8, HEAD_DIM), F32),
                 vmem((seqs - 1, rows, width), BF16),
                 vmem((length, width), BF16),
@@ -613,7 +628,6 @@
                 vmem((2, seqs, HEAD_DIM, HEAD_DIM), BF16),
                 vmem((seqs, length, 2 * HEAD_DIM), BF16),
                 vmem((seqs, rows, HEAD_DIM * tp), BF16),
-                vmem((seqs * rows, width), F32),
                 dma(()), dma(()), dma((seqs, 4)), dma((2,)), dma(()), dma((6,)), dma(()),
                 dma((3,)), dma((seqs,)), dma((seqs,)), dma((seqs,)), dma(()), dma((2, seqs)),
                 dma((8,)), dma(()), dma((seqs,)), pltpu.SemaphoreType.REGULAR,
@@ -629,12 +643,12 @@
         return pl.pallas_call(
             hand_over,
             out_shape=jax.ShapeDtypeStruct(tok.shape, BF16),
-            in_specs=[pl.BlockSpec(memory_space=pltpu.VMEM)],
+            in_specs=[pl.BlockSpec(memory_space=pltpu.VMEM)] * 3,
             out_specs=hbm,
-            scratch_shapes=[dma(())],
+            scratch_shapes=[vmem((rows, width), BF16), dma((2,))],
             compiler_params=pltpu.CompilerParams(vmem_limit_bytes=16 * 2**20),
             name="hand_over",
-        )(mixed)
+        )(mixed, premix, post)
 
     placed = (
         P(None, ("sp", "tp"), None),

time: 50.9 us -> 50.6 us (level)
  no operation moved by 1% of the time
where the time goes in v7:
time: 50.6 us; the launch traced here: 50.4 us
  Pallas kernels  49.8 us (98%)
  between operations  0.66 us (1%)
    pallas_call x1, Pallas kernels, body(): pl.pallas_call(functools.partial(kernel, tp, sp), out_shape=(jax.ShapeDty...  48.8 us

profile of v7, /device:TPU:227, one launch (start us, length us, event | category | flops | bytes accessed | tf_op | source)
XLA Modules:
  0.0 50.4 jit_solution(18015412078989660134)
XLA Ops:
  0.7 48.8 %retention.1 = (bf16[4,64,2048]{2,1,0:T(8,128)(2,1)S(1)}, f32[256,2048]{1,0:T(8,128)S(1)}, f32[1,2048]{1,0:T(1,128)S(1)}) custom-call(bf16[4,64,2048]{2,1,0:T(8,128)(2,1)} %tok.1, f32[1,2048]{1,0:T(1,128)} %bitcast.3, bf16[2048,128]{1,0:T(8,128)(2,1)} %wq_h.1, bf16[2048,128]{1,0:T(8,128)(2,1)} %wk_h.1, bf16[2048,128]{1,0:T(8,128)(2,1)} %wv_h.1, ...), custom_call_target="tpu_custom_call" | custom-call | tf_op jit(solution)/shard_map/retention/pallas_call | solution.py:597
  49.5 1.0 %hand_over.1 = bf16[4,64,2048]{2,1,0:T(8,128)(2,1)} custom-call(bf16[4,64,2048]{2,1,0:T(8,128)(2,1)S(1)} %get-tuple-element.8.source, f32[256,2048]{1,0:T(8,128)S(1)} %get-tuple-element.9.premix, f32[1,2048]{1,0:T(1,128)S(1)} %get-tuple-element.10.pgain), custom_call_target="tpu_custom_call" | custom-call | tf_op jit(solution)/shard_map/hand_over/pallas_call | solution.py:643

commit v8 on v7

--- a/solution.py
+++ b/solution.py
@@ -62,11 +62,11 @@
 
     cuts = [slice(i * HEAD_DIM, (i + 1) * HEAD_DIM) for i in range(4)]
     loads_w = [
-        pltpu.make_async_copy(a, w.at[0, :, cuts[i]], w_sem.at[i])
+        pltpu.make_async_copy(a, w.at[0, :, cuts[i]], w_sem.at[0])
         for i, a in enumerate((wk_h, wv_h, wq_h, wg_h))
     ]
     loads = [
-        pltpu.make_async_copy(a, b, w_sem.at[4 + i])
+        pltpu.make_async_copy(a, b, w_sem.at[1 + i])
         for i, (a, b) in enumerate(
             ((ngain_h, heads.at[0, 1:2, :]), (gain_h, gain), (inv_h, inv), (pgain_h, pgain))
         )
@@ -140,15 +140,15 @@
             heads.at[0], heads.at[1], w_send, h_recv, device_id={"tp": mirror}, device_id_type=MESH,
         )
 
-    def block_copy(q, u, dest, sem):
+    def block_copy(q, u, dest, sem, kind):
         held = raw.at[at_rows(u, rows), :] if q is None else gath.at[q, at_rows(u, rows), :]
         return pltpu.make_async_remote_copy(
-            held, held, sem, t_recv.at[0 if q is None else q, u],
+            held, held, sem, t_recv.at[(0 if q is None else q) * 3 + kind],
             device_id={"tp": base + dest}, device_id_type=MESH,
         )
 
-    def arrived(q, u):
-        block_copy(q, u, twin, x_send).wait_recv()
+    def arrived(q, u, kind):
+        block_copy(q, u, twin, x_send, kind).wait_recv()
 
     def normalise(source, q, u):
         def norm(i, _):
@@ -168,8 +168,8 @@
         normalise(lambda at: raw[pl.ds(pl.multiple_of(u * rows + at, 16), 16), :], 0, u)
 
     def send(q):
-        block_copy(q, me, across, x_send).start()
-        block_copy(q, me, twin, p_send).start()
+        block_copy(q, me, across, x_send, 1).start()
+        block_copy(q, me, twin, p_send, 0).start()
 
     def last_copy(u, late, dest, sem, arrival):
         span = pl.ds(pl.multiple_of(u * rows + late * (rows - 16), 16), 16 if late else rows - 16)
@@ -182,7 +182,7 @@
         for late in range(2):
             with jax.named_scope("takelast"):
                 last_copy(across, late, twin, p_send, last_recv.at[late]).wait_recv()
-            last_copy(across, late, twin, p_send, t_recv.at[seqs - 1, across]).start()
+            last_copy(across, late, twin, p_send, t_recv.at[3 * seqs - 1]).start()
 
     with jax.named_scope("load0"):
         loads_in[0].wait()
@@ -190,8 +190,8 @@
         load.start()
     with jax.named_scope("barrier"):
         pl.semaphore_wait(barrier, 3 + NY - 1 + NY + z)
-    block_copy(None, me, across, x_send).start()
-    block_copy(None, me, twin, p_send).start()
+    block_copy(None, me, across, x_send, 1).start()
+    block_copy(None, me, twin, p_send, 0).start()
     for d in range(1, nz):
         @pl.when(z >= d)
         def _():
@@ -207,8 +207,10 @@
         head_copy().start()
         norm_own(2)
         send(1)
+        pltpu.make_async_remote_copy(
+            w.at[0], w.at[0], w_sem.at[0], h_recv, device_id={"tp": mirror}, device_id_type=MESH,
+        ).wait_send()
         for i in range(4):
-            loads_w[i].wait()
             cross(i).start()
         for i in range(4):
             straight(i).start()
@@ -219,7 +221,7 @@
         send(2)
         for late in range(2):
             last_copy(me, late, across, x_send, last_recv.at[late]).start()
-        block_copy(seqs - 1, me, twin, p_send).start()
+        block_copy(seqs - 1, me, twin, p_send, 0).start()
 
     with jax.named_scope("tables"):
         loads[2].wait()
@@ -358,7 +360,7 @@
     def gated_copy(q, dest, source, near_by=0):
         return pltpu.make_async_remote_copy(
             g_out.at[q, at_rows(dest, rows), :], g_in.at[q, :, at_rows(source, 2 * HEAD_DIM)],
-            g_send, g_recv.at[near_by, q],
+            g_send, g_recv.at[q + near_by * lax.div(q, seqs - 1)],
             device_id={"tp": base + dest}, device_id_type=MESH,
         )
 
@@ -385,9 +387,9 @@
                 g_in[q, :, at_rows(me, 2 * HEAD_DIM)] = g_out[q, at_rows(me, rows), :]
 
     def gated_wait(q, near_by):
-        took = g_in.at[q, :, 0:(2 if near_by else 4) * HEAD_DIM]
+        took = g_in.at[q, :, 0:(2 if near_by else 4 if q == seqs - 1 else 6) * HEAD_DIM]
         pltpu.make_async_remote_copy(
-            took, took, g_send, g_recv.at[near_by, q],
+            took, took, g_send, g_recv.at[q + near_by],
             device_id={"tp": mirror}, device_id_type=MESH,
         ).wait_recv()
 
@@ -411,7 +413,6 @@
         with jax.named_scope("gated_wait"):
             for q in range(lo, hi):
                 gated_wait(q, 0)
-                gated_wait(q, 1)
         g = g_in[lo:hi].reshape(n, g_in.shape[2])
         for c in range(width // step):
             cut = slice(c * step, (c + 1) * step)
@@ -441,31 +442,31 @@
         lax.fori_loop(lo, hi, run, 0)
 
     def near(q):
-        arrived(q, twin)
+        arrived(q, twin, 0)
         project_kv(0, q, own_rows)
         project_qg(0, q, own_rows)
 
     def near_raw():
-        arrived(None, twin)
+        arrived(None, twin, 0)
         norm_raw(twin)
         project_kv(0, 0, own_rows)
         project_qg(0, 0, own_rows)
 
     def take(q):
         with jax.named_scope("take"):
-            arrived(q, across)
-        block_copy(q, across, twin, p_send).start()
+            arrived(q, across, 1)
+        block_copy(q, across, twin, p_send, 2).start()
 
     def rest(q):
         with jax.named_scope("take2"):
-            arrived(q, across_twin)
+            arrived(q, across_twin, 2)
         project_kv(0, q, far_rows)
         project_qg(0, q, far_rows)
 
     def rest_raw():
         norm_raw(across)
         with jax.named_scope("take2"):
-            arrived(None, across_twin)
+            arrived(None, across_twin, 2)
         norm_raw(across_twin)
         project_kv(0, 0, far_rows)
         project_qg(0, 0, far_rows)
@@ -518,7 +519,7 @@
     project_qg(1, end, own_rows)
     scoped("plane1", plane_total, 1)
     with jax.named_scope("take2e"):
-        arrived(end, across_twin)
+        arrived(end, across_twin, 2)
     with jax.named_scope("rest3"):
         for h in range(2):
             project_kv(h, end, far_rows)
@@ -628,9 +629,9 @@
                 vmem((2, seqs, HEAD_DIM, HEAD_DIM), BF16),
                 vmem((seqs, length, 2 * HEAD_DIM), BF16),
                 vmem((seqs, rows, HEAD_DIM * tp), BF16),
-                dma(()), dma(()), dma((seqs, 4)), dma((2,)), dma(()), dma((6,)), dma(()),
-                dma((3,)), dma((seqs,)), dma((seqs,)), dma((seqs,)), dma(()), dma((2, seqs)),
-                dma((8,)), dma(()), dma((seqs,)), pltpu.SemaphoreType.REGULAR,
+                dma(()), dma(()), dma((3 * seqs,)), dma((2,)), dma(()), dma((6,)), dma(()),
+                dma((3,)), dma((seqs,)), dma((seqs,)), dma((seqs,)), dma(()), dma((seqs + 1,)),
+                dma((5,)), dma(()), dma((seqs,)), pltpu.SemaphoreType.REGULAR,
             ],
             compiler_params=pltpu.CompilerParams(
                 collective_id=0, has_side_effects=True, vmem_limit_bytes=40 * 2**20

time: 50.6 us -> 50.7 us (level)
  no operation moved by 1% of the time
where the time goes in v8:
time: 50.7 us; the launch traced here: 50.6 us
  Pallas kernels  49.9 us (98%)
  between operations  0.66 us (1%)
    pallas_call x1, Pallas kernels, body(): pl.pallas_call(functools.partial(kernel, tp, sp), out_shape=(jax.ShapeDty...  48.9 us

profile of v8, /device:TPU:227, one launch (start us, length us, event | category | flops | bytes accessed | tf_op | source)
XLA Modules:
  0.0 50.6 jit_solution(2600050211420008109)
XLA Ops:
  0.7 48.9 %retention.1 = (bf16[4,64,2048]{2,1,0:T(8,128)(2,1)S(1)}, f32[256,2048]{1,0:T(8,128)S(1)}, f32[1,2048]{1,0:T(1,128)S(1)}) custom-call(bf16[4,64,2048]{2,1,0:T(8,128)(2,1)} %tok.1, f32[1,2048]{1,0:T(1,128)} %bitcast.3, bf16[2048,128]{1,0:T(8,128)(2,1)} %wq_h.1, bf16[2048,128]{1,0:T(8,128)(2,1)} %wk_h.1, bf16[2048,128]{1,0:T(8,128)(2,1)} %wv_h.1, ...), custom_call_target="tpu_custom_call" | custom-call | tf_op jit(solution)/shard_map/retention/pallas_call | solution.py:598
  49.6 1.0 %hand_over.1 = bf16[4,64,2048]{2,1,0:T(8,128)(2,1)} custom-call(bf16[4,64,2048]{2,1,0:T(8,128)(2,1)S(1)} %get-tuple-element.8.source, f32[256,2048]{1,0:T(8,128)S(1)} %get-tuple-element.9.premix, f32[1,2048]{1,0:T(1,128)S(1)} %get-tuple-element.10.pgain), custom_call_target="tpu_custom_call" | custom-call | tf_op jit(solution)/shard_map/hand_over/pallas_call | solution.py:644

commit v9 on v8

--- a/solution.py
+++ b/solution.py
@@ -538,7 +538,8 @@
     scoped("back3", hand_back, end)
     scoped("finish01", over, 0, 2, finish)
     scoped("finish23", over, 2, seqs, finish)
-    scoped("emit0", emit, 0, end)
+    scoped("emit0", emit, 0, 2)
+    scoped("emit2", emit, 2, end)
     scoped("emit3a", emit_half, end, seqs, side, 1)
     scoped("emit3b", emit_half, end, seqs, 1 - side, 0)
 

time: 50.7 us -> 50.7 us (level)
  no operation moved by 1% of the time
where the time goes in v9:
time: 50.7 us; the launch traced here: 50.3 us
  Pallas kernels  49.7 us (98%)
  between operations  0.66 us (1%)
    pallas_call x1, Pallas kernels, body(): pl.pallas_call(functools.partial(kernel, tp, sp), out_shape=(jax.ShapeDty...  48.7 us

profile of v9, /device:TPU:227, one launch (start us, length us, event | category | flops | bytes accessed | tf_op | source)
XLA Modules:
  0.0 50.3 jit_solution(5751236631566610949)
XLA Ops:
  0.7 48.7 %retention.1 = (bf16[4,64,2048]{2,1,0:T(8,128)(2,1)S(1)}, f32[256,2048]{1,0:T(8,128)S(1)}, f32[1,2048]{1,0:T(1,128)S(1)}) custom-call(bf16[4,64,2048]{2,1,0:T(8,128)(2,1)} %tok.1, f32[1,2048]{1,0:T(1,128)} %bitcast.3, bf16[2048,128]{1,0:T(8,128)(2,1)} %wq_h.1, bf16[2048,128]{1,0:T(8,128)(2,1)} %wk_h.1, bf16[2048,128]{1,0:T(8,128)(2,1)} %wv_h.1, ...), custom_call_target="tpu_custom_call" | custom-call | tf_op jit(solution)/shard_map/retention/pallas_call | solution.py:599
  49.3 1.0 %hand_over.1 = bf16[4,64,2048]{2,1,0:T(8,128)(2,1)} custom-call(bf16[4,64,2048]{2,1,0:T(8,128)(2,1)S(1)} %get-tuple-element.8.source, f32[256,2048]{1,0:T(8,128)S(1)} %get-tuple-element.9.premix, f32[1,2048]{1,0:T(1,128)S(1)} %get-tuple-element.10.pgain), custom_call_target="tpu_custom_call" | custom-call | tf_op jit(solution)/shard_map/hand_over/pallas_call | solution.py:645
